TPU v7x, 128 devices: a whole 4x4x4 slice. The times are simulated.
128 devices in a mesh: sp: 16 (over z, x), tp: 8 (over y, core).
Axes of the slice: x: 4, y: 4, z: 4, core: 2. Of those that a mesh axis runs over, the one named last changes fastest.
Arguments:
- block_input: bfloat16 [32768, 4096], P('sp'), may hold values from -6 to 6
- value_weight: bfloat16 [4096, 1024], P(None, 'tp'), may hold values from -0.09375 to 0.09375
- key_rows: bfloat16 [32768, 512], P('sp', 'tp'), may hold values from -1 to 1
- query_rows: bfloat16 [32768, 512], P('sp', 'tp'), may hold values from -1 to 1
- decay_pre: float32 [16, 32768], P('tp', 'sp'), may hold values from -3 to 2
- decay_log: float32 [16], P('tp'), may hold values from -16 to -2
- gate_rows: bfloat16 [32768, 1024], P('sp', 'tp'), may hold values from -6 to 6
- out_grad: bfloat16 [32768, 1024], P('sp', 'tp'), may hold values from -6 to 6
Outputs:
- key_grad: float32 [32768, 512], P('sp', 'tp')
- query_grad: float32 [32768, 512], P('sp', 'tp')
- decay_grad: float32 [16, 32768], P('tp', 'sp')
- gate_grad: float32 [32768, 1024], P('sp', 'tp')
- weight_grad: float32 [4096, 1024], P('sp', 'tp')
- row_norms: float32 [4096], P('sp')
All inputs are finite; a program needn't handle non-finite values.
Results may differ from a plain program's by a relative error of at most 0.0035.
Values sent between devices are 32-bit elements; how exact they have to be, the bound alone decides.
A program may use at most 128 MiB of HBM per device.

v0:
```python
import functools

import jax
import jax.numpy as jnp
from jax import lax
from jax.experimental import pallas as pl
from jax.experimental.pallas import tpu as pltpu
from jax.sharding import PartitionSpec as P

HEAD = 64
STATE = 64
BLK = 128
RING = 4
F32 = jnp.float32
BF16 = jnp.bfloat16
HIGHEST = lax.Precision.HIGHEST
MESH = pl.DeviceIdType.MESH

ORDER = [
    (2, 2), (2, 0), (0, 2), (2, 1), (1, 2), (2, 3), (3, 2), (1, 3),
    (3, 1), (3, 3), (1, 1), (1, 0), (0, 1), (3, 0), (0, 3), (0, 0),
]


def nn(a, b, precision=None):
    return lax.dot_general(a, b, (((1,), (0,)), ((), ())), precision=precision, preferred_element_type=F32)


def nt(a, b, precision=None):
    return lax.dot_general(a, b, (((1,), (1,)), ((), ())), precision=precision, preferred_element_type=F32)


def tn(a, b, precision=None):
    return lax.dot_general(a, b, (((0,), (0,)), ((), ())), precision=precision, preferred_element_type=F32)


def halves(a):
    high = a.astype(BF16)
    return high, (a - high.astype(F32)).astype(BF16)


def both(a):
    return jnp.concatenate(halves(a), axis=1)


def folded(a):
    width = a.shape[1] // 2
    return a[:, :width] + a[:, width:]


def softplus(a):
    return jnp.maximum(a, 0.0) + jnp.log1p(jnp.exp(-jnp.abs(a)))


def sigmoid(a):
    return 1.0 / (1.0 + jnp.exp(-a))


def mixer(
    sp_count,
    tp_count,
    x_hbm, w_hbm, k_hbm, q_hbm, pre_hbm, rate_ref, gate_hbm, cot_hbm,
    kg_ref, qg_ref, dg_ref, gg_ref, wg_ref, rn_ref,
    x_v, w_v, k_v, q_v, pre_v, gate_v, cot_v,
    rows_s, stack_s, rend_s,
    dy_s, tm_s, lm_s, er_s, te_s, se_s, p_s, v_s, u_s,
    gst_s, sst_s, bs_s, out_s, inc_s, vgt_s,
    yy_s, dd_s, ee_s,
    gmsg, smsg, gslots, sslots,
    part, far_r, near_r, red_s, far2_r, near2_r,
    nmsg, nslots,
    in_sem, x_sem, gs_sem, gr_sem, ss_sem, sr_sem,
    fs_sem, fr_sem, ns_sem, nr_sem, f2s_sem, f2r_sem, n2s_sem, n2r_sem, norm_s, norm_r,
):
    tokens, width = x_v.shape
    blocks = tokens // BLK
    lanes = 2 * HEAD
    cols = width // sp_count
    me = lax.axis_index("sp")
    my_tp = lax.axis_index("tp")
    mz, mx = lax.div(me, RING), lax.rem(me, RING)

    barrier = pltpu.get_barrier_semaphore()
    for off in range(1, sp_count):
        pl.semaphore_signal(
            barrier, inc=1, device_id={"sp": lax.rem(me + off, sp_count)}, device_id_type=MESH
        )
    for off in range(1, tp_count):
        pl.semaphore_signal(
            barrier, inc=1, device_id={"tp": lax.rem(my_tp + off, tp_count)}, device_id_type=MESH
        )

    small = [
        pltpu.make_async_copy(src, dst, in_sem.at[i])
        for i, (src, dst) in enumerate(
            [(pre_hbm, pre_v), (q_hbm, q_v), (k_hbm, k_v), (gate_hbm, gate_v), (cot_hbm, cot_v), (w_hbm, w_v)]
        )
    ]
    for copy in small:
        copy.start()
    xrows = 2 * BLK
    xchunks = tokens // xrows

    def x_copy(i):
        rows = pl.ds(pl.multiple_of(i * xrows, xrows), xrows)
        return pltpu.make_async_copy(x_hbm.at[rows], x_v.at[rows], x_sem.at[i])

    for i in range(xchunks):
        x_copy(i).start()

    small[0].wait()
    for h in range(2):
        for c in range(blocks):
            rows_s[h * blocks + c : h * blocks + c + 1, :] = pre_v[h : h + 1, c * BLK : (c + 1) * BLK]
    pre = rows_s[...]
    row_id = lax.broadcasted_iota(jnp.int32, (2 * blocks, BLK), 0)
    rate = jnp.where(
        row_id < blocks,
        jnp.exp(jnp.full((2 * blocks, BLK), rate_ref[0], F32)),
        jnp.exp(jnp.full((2 * blocks, BLK), rate_ref[1], F32)),
    )
    step = softplus(pre)
    sq_row = lax.broadcasted_iota(jnp.int32, (BLK, BLK), 0)
    sq_col = lax.broadcasted_iota(jnp.int32, (BLK, BLK), 1)
    lower = sq_row >= sq_col
    run = nn(-rate * step, (sq_row <= sq_col).astype(F32), HIGHEST)
    stack_s[...] = jnp.zeros_like(stack_s)
    stack_s[0 : 2 * blocks, :] = run
    stack_s[2 * blocks : 4 * blocks, :] = step
    turned = stack_s[...].T
    first_head = lax.broadcasted_iota(jnp.int32, (BLK, lanes), 1) < HEAD
    first_lane = lax.broadcasted_iota(jnp.int32, (STATE, lanes), 1) < HEAD
    for copy in small[1:5]:
        copy.wait()

    def prepare(c, carry):
        rows = pl.ds(pl.multiple_of(c * BLK, BLK), BLK)
        rolled = pltpu.roll(turned, lax.rem(BLK - c, BLK), 1)
        col = [jnp.broadcast_to(rolled[:, i * blocks : i * blocks + 1], (BLK, BLK)) for i in range(4)]
        scores = nt(q_v[rows, :], k_v[rows, :])
        for h in range(2):
            row = stack_s[pl.ds(h * blocks + c, 1), :]
            decay = jnp.exp(jnp.where(lower, col[h] - row, -1e30))
            lm_s[rows, h * BLK : (h + 1) * BLK] = decay
            tm_s[rows, h * BLK : (h + 1) * BLK] = scores * decay
        running = jnp.where(first_head, col[0], col[1])
        end = running[BLK - 1 : BLK, :]
        er = jnp.exp(running)
        er_s[rows, :] = er
        te_s[rows, :] = jnp.exp(end - running)
        se_s[rows, :] = jnp.where(first_head, col[2], col[3])
        rend_s[pl.ds(c, 1), :] = end
        gate = gate_v[rows, :].astype(F32)
        dy = cot_v[rows, :].astype(F32) * gate * sigmoid(gate)
        dy_s[rows, :] = dy
        bs_s[c] = folded(tn(q_v[rows, :], both(er * dy)))
        return carry

    lax.fori_loop(0, blocks, prepare, 0)
    grad = jnp.zeros((STATE, lanes), F32)
    total = jnp.zeros((1, lanes), F32)
    for c in reversed(range(blocks)):
        end = rend_s[c : c + 1, :]
        grad = jnp.exp(end) * grad + bs_s[c]
        total = total + end
        gst_s[c] = grad
    gmsg[0:STATE, :] = grad
    gmsg[STATE : STATE + 8, :] = jnp.broadcast_to(total, (8, lanes))

    def state_copy(msg, slots, send, recv, source, target):
        return pltpu.make_async_remote_copy(
            src_ref=msg,
            dst_ref=slots.at[source],
            send_sem=send.at[target],
            recv_sem=recv.at[source],
            device_id={"sp": target},
            device_id_type=MESH,
        )

    pl.semaphore_wait(barrier, sp_count + tp_count - 2)
    for target in range(sp_count - 1):

        @pl.when(target < me)
        def _(target=target):
            state_copy(gmsg, gslots, gs_sem, gr_sem, me, target).start()

    small[5].wait()

    def project(i, carry):
        x_copy(i).wait()
        rows = pl.ds(pl.multiple_of(i * xrows, xrows), xrows)
        projected = nn(x_v[rows, :], w_v[...]).astype(BF16).astype(F32)
        p_s[rows, :] = projected
        v_s[rows, :] = projected * sigmoid(projected)
        for b in range(xrows // BLK):
            c = i * (xrows // BLK) + b
            rows = pl.ds(pl.multiple_of(c * BLK, BLK), BLK)
            bs_s[c] = folded(tn(k_v[rows, :], both(te_s[rows, :] * se_s[rows, :] * v_s[rows, :])))
            dy_high, dy_low = halves(dy_s[rows, :])
            t_high, t_low = halves(tm_s[rows, :])
            u = folded(tn(t_high, jnp.concatenate([dy_high, dy_low], axis=1))) + tn(t_low, dy_high)
            u_s[rows, :] = jnp.where(first_head, u[0:BLK, :], u[BLK : 2 * BLK, :])
        return carry

    lax.fori_loop(0, xchunks, project, 0)
    state = jnp.zeros((STATE, lanes), F32)
    for c in range(blocks):
        sst_s[c] = state
        state = jnp.exp(rend_s[c : c + 1, :]) * state + bs_s[c]
    smsg[0:STATE, :] = state
    smsg[STATE : STATE + 8, :] = jnp.broadcast_to(total, (8, lanes))
    for target in range(1, sp_count):

        @pl.when(target > me)
        def _(target=target):
            state_copy(smsg, sslots, ss_sem, sr_sem, me, target).start()

    out_s[...] = jnp.zeros_like(out_s)
    for source in reversed(range(1, sp_count)):

        @pl.when(source > me)
        def _(source=source):
            state_copy(gmsg, gslots, gs_sem, gr_sem, source, me).wait_recv()
            out_s[...] = gslots[source, 0:STATE, :] + jnp.exp(gslots[source, STATE : STATE + 1, :]) * out_s[...]

    after = jnp.zeros((1, lanes), F32)
    for c in reversed(range(blocks)):
        after = after + rend_s[c : c + 1, :]
        gst_s[c] = gst_s[c] + jnp.exp(after) * out_s[...]
    gst_s[blocks] = out_s[...]

    def value_gradient(c, carry):
        rows = pl.ds(pl.multiple_of(c * BLK, BLK), BLK)
        u = u_s[rows, :] + te_s[rows, :] * folded(nn(k_v[rows, :], both(gst_s[c + 1])))
        u_s[rows, :] = u
        projected = p_s[rows, :]
        sig = sigmoid(projected)
        vg = se_s[rows, :] * u * sig * (1.0 + projected * (1.0 - sig))
        vgt_s[:, rows] = vg.T.astype(BF16)
        return carry

    lax.fori_loop(0, blocks, value_gradient, 0)

    def owner(dz, dx):
        return lax.rem(mz + dz, RING) * RING + lax.rem(mx + dx, RING)

    def neighbour(half, stage, direction):
        if half == stage:
            return lax.rem(mz + direction + RING, RING) * RING + mx
        return mz * RING + lax.rem(mx + direction + RING, RING)

    def half_of(half, dz, dx):
        return part.at[owner(dz, dx), half * HEAD : (half + 1) * HEAD, :]

    def piece(half, dist, across):
        return half_of(half, dist, across) if half == 0 else half_of(half, across, dist)

    def far_copy(half, across):
        direction = 1 if across < 2 else -1
        slot = half * RING + across
        return pltpu.make_async_remote_copy(
            src_ref=piece(half, 2, across),
            dst_ref=far_r.at[slot],
            send_sem=fs_sem.at[slot],
            recv_sem=fr_sem.at[slot],
            device_id={"sp": neighbour(half, 0, direction)},
            device_id_type=MESH,
        )

    def near_copy(half, direction, across):
        slot = (half * 2 + (0 if direction == 1 else 1)) * RING + across
        return pltpu.make_async_remote_copy(
            src_ref=piece(half, 1 if direction == 1 else 3, across),
            dst_ref=near_r.at[slot],
            send_sem=ns_sem.at[slot],
            recv_sem=nr_sem.at[slot],
            device_id={"sp": neighbour(half, 0, direction)},
            device_id_type=MESH,
        )

    for dz, dx in ORDER:
        dest = owner(dz, dx)
        columns = pl.ds(pl.multiple_of(dest * cols, cols), cols)
        part[dest] = nn(vgt_s[...], x_v[:, columns])
        for half, dist, across in ((0, dz, dx), (1, dx, dz)):
            if dist == 2:
                far_copy(half, across).start()
            elif dist == 1 and across >= 2:
                near_copy(half, 1, across).start()
            elif dist == 3 and across < 2:
                near_copy(half, -1, across).start()
    for across in range(2):
        for half in range(2):
            for direction, lane in ((1, across), (-1, across + 2)):
                far_copy(half, lane).wait_recv()
                ref = piece(half, 1 if direction == 1 else 3, lane)
                ref[...] = ref[...] + far_r[half * RING + lane]
                near_copy(half, direction, lane).start()

    inc_s[...] = jnp.zeros_like(inc_s)
    for source in range(sp_count - 1):

        @pl.when(source < me)
        def _(source=source):
            state_copy(smsg, sslots, ss_sem, sr_sem, source, me).wait_recv()
            inc_s[...] = sslots[source, 0:STATE, :] + jnp.exp(sslots[source, STATE : STATE + 1, :]) * inc_s[...]

    before = jnp.zeros((1, lanes), F32)
    for c in range(blocks):
        full = sst_s[c] + jnp.exp(before) * inc_s[...]
        sst_s[c] = full
        before = before + rend_s[c : c + 1, :]
        if c > 0:
            ee_s[c - 1 : c, :] = jnp.sum(full * gst_s[c], axis=0, keepdims=True)
    last = smsg[0:STATE, :] + jnp.exp(before) * inc_s[...]
    ee_s[blocks - 1 : blocks, :] = jnp.sum(last * gst_s[blocks], axis=0, keepdims=True)

    head_of = lax.broadcasted_iota(jnp.int32, (8, lanes), 0)
    lane_head = lax.div(lax.broadcasted_iota(jnp.int32, (8, lanes), 1), HEAD)
    pick = (head_of == lane_head).astype(BF16)
    zero = jnp.zeros((BLK, lanes), BF16)

    def head_rows(a):
        high, low = halves(a)
        return nt(pick, high) + nt(pick, low)

    def others(c, carry):
        rows = pl.ds(pl.multiple_of(c * BLK, BLK), BLK)
        q, k = q_v[rows, :], k_v[rows, :]
        dy, v, u, er, te = dy_s[rows, :], v_s[rows, :], u_s[rows, :], er_s[rows, :], te_s[rows, :]
        sv = se_s[rows, :] * v
        sv_high, sv_low = halves(sv)
        dy_high, dy_low = halves(dy)

        def split_heads(a, axis):
            return jnp.concatenate([jnp.where(first_head, a, zero), jnp.where(first_head, zero, a)], axis=axis)

        t_high, t_low = halves(tm_s[rows, :])
        spread_high = split_heads(sv_high, 0)
        mixed = folded(nn(t_high, jnp.concatenate([spread_high, split_heads(sv_low, 0)], axis=1)))
        mixed = mixed + nn(t_low, spread_high)
        mixed = mixed + er * folded(nn(q, both(sst_s[c])))
        gate = gate_v[rows, :].astype(F32)
        sig = sigmoid(gate)
        gg_ref[rows, :] = cot_v[rows, :].astype(F32) * mixed * sig * (1.0 + gate * (1.0 - sig))
        by_head = split_heads(dy_high, 0)
        dp = nt(jnp.concatenate([by_head, split_heads(dy_low, 0)], axis=1), jnp.concatenate([sv_high, sv_high], axis=1))
        dp = dp + nt(by_head, sv_low)
        d = dp[0:BLK, :] * lm_s[rows, 0:BLK] + dp[BLK : 2 * BLK, :] * lm_s[rows, BLK : 2 * BLK]
        d_high, d_low = halves(d)
        es_high, es_low = halves(er * dy)
        s_high, s_low = halves(sst_s[c])
        qg_ref[rows, :] = (
            nn(d_high, k) + nn(d_low, k) + nt(es_high, s_high) + nt(es_low, s_high) + nt(es_high, s_low)
        )
        ts_high, ts_low = halves(te * sv)
        g_high, g_low = halves(gst_s[c + 1])
        kg_ref[rows, :] = (
            tn(d_high, q) + tn(d_low, q) + nt(ts_high, g_high) + nt(ts_low, g_high) + nt(ts_high, g_low)
        )
        yy = head_rows(dy * mixed)
        dd = head_rows(v * u)
        for h in range(2):
            yy_s[pl.ds(h * blocks + c, 1), :] = yy[h : h + 1, :]
            dd_s[pl.ds(h * blocks + c, 1), :] = dd[h : h + 1, :]
        return carry

    half_way = blocks // 2
    lax.fori_loop(0, half_way, others, 0)

    quarter = HEAD // 2

    def total_of(half, across):
        plus, minus = (half * 2) * RING + across, (half * 2 + 1) * RING + across
        near_copy(half, 1, across).wait_recv()
        near_copy(half, -1, across).wait_recv()
        return piece(half, 0, across)[...] + near_r[plus] + near_r[minus]

    def far2_copy(half, which):
        slot = half * 2 + which
        return pltpu.make_async_remote_copy(
            src_ref=red_s.at[half * RING + 2, which * quarter : (which + 1) * quarter, :],
            dst_ref=far2_r.at[slot],
            send_sem=f2s_sem.at[slot],
            recv_sem=f2r_sem.at[slot],
            device_id={"sp": neighbour(half, 1, 1 if which == 0 else -1)},
            device_id_type=MESH,
        )

    def near2_copy(half, direction, which):
        side = 0 if direction == 1 else 1
        slot = (half * 2 + side) * 2 + which
        return pltpu.make_async_remote_copy(
            src_ref=red_s.at[half * RING + (1 if direction == 1 else 3), which * quarter : (which + 1) * quarter, :],
            dst_ref=near2_r.at[slot],
            send_sem=n2s_sem.at[slot],
            recv_sem=n2r_sem.at[slot],
            device_id={"sp": neighbour(half, 1, direction)},
            device_id_type=MESH,
        )

    for across in (2, 1, 3, 0):
        for half in range(2):
            red_s[half * RING + across] = total_of(half, across)
            if across == 2:
                far2_copy(half, 0).start()
                far2_copy(half, 1).start()
            elif across == 1:
                near2_copy(half, 1, 1).start()
            elif across == 3:
                near2_copy(half, -1, 0).start()
    for half in range(2):
        for direction, which in ((1, 0), (-1, 1)):
            far2_copy(half, which).wait_recv()
            at = half * RING + (1 if direction == 1 else 3)
            span = slice(which * quarter, (which + 1) * quarter)
            red_s[at, span, :] = red_s[at, span, :] + far2_r[half * 2 + which]
            near2_copy(half, direction, which).start()

    lax.fori_loop(half_way, blocks, others, 0)

    ends = ee_s[...]
    end_cols = jnp.concatenate(
        [
            jnp.sum(ends[:, 0:HEAD], axis=1, keepdims=True),
            jnp.sum(ends[:, HEAD:lanes], axis=1, keepdims=True),
        ],
        axis=0,
    )
    direct = dd_s[...]
    log_grad = nn(yy_s[...] - step * direct, lower.astype(F32), HIGHEST) + end_cols
    decay_grad = (direct - rate * log_grad) * sigmoid(pre)
    for h in range(2):
        for c in range(blocks):
            dg_ref[h : h + 1, c * BLK : (c + 1) * BLK] = decay_grad[h * blocks + c : h * blocks + c + 1, :]

    squares = jnp.zeros((1, cols), F32)
    for half in range(2):
        for which in range(2):
            for direction in (1, -1):
                near2_copy(half, direction, which).wait_recv()
            plus, minus = (half * 2) * 2 + which, (half * 2 + 1) * 2 + which
            span = slice(which * quarter, (which + 1) * quarter)
            done = red_s[half * RING, span, :] + near2_r[plus] + near2_r[minus]
            red_s[half * RING, span, :] = done
            squares = squares + jnp.sum(done * done, axis=0, keepdims=True)

    def norm_copy(source, target):
        return pltpu.make_async_remote_copy(
            src_ref=nmsg,
            dst_ref=nslots.at[source],
            send_sem=norm_s.at[target],
            recv_sem=norm_r.at[source],
            device_id={"tp": target},
            device_id_type=MESH,
        )

    nmsg[...] = jnp.broadcast_to(squares, (8, cols))
    for off in range(1, tp_count):
        norm_copy(my_tp, lax.rem(my_tp + off, tp_count)).start()
    for half in range(2):
        wg_ref[:, half * HEAD : (half + 1) * HEAD] = red_s[half * RING].T
    norms = squares
    for off in range(1, tp_count):
        source = lax.rem(my_tp + off, tp_count)
        norm_copy(source, my_tp).wait_recv()
        norms = norms + nslots[source, 0:1, :]
    rn_ref[...] = norms

    for target in range(sp_count - 1):

        @pl.when(target < me)
        def _(target=target):
            state_copy(gmsg, gslots, gs_sem, gr_sem, me, target).wait_send()

    for target in range(1, sp_count):

        @pl.when(target > me)
        def _(target=target):
            state_copy(smsg, sslots, ss_sem, sr_sem, me, target).wait_send()

    for half in range(2):
        for across in range(RING):
            far_copy(half, across).wait_send()
            for direction in (1, -1):
                near_copy(half, direction, across).wait_send()
        for which in range(2):
            far2_copy(half, which).wait_send()
            for direction in (1, -1):
                near2_copy(half, direction, which).wait_send()
    for off in range(1, tp_count):
        norm_copy(my_tp, lax.rem(my_tp + off, tp_count)).wait_send()


def shards(sp_count, tp_count, block_input, value_weight, key_rows, query_rows, decay_pre, decay_log, gate_rows, out_grad):
    tokens, width = block_input.shape
    blocks = tokens // BLK
    lanes = 2 * HEAD
    cols = width // sp_count
    vmem = lambda shape, dtype=F32: pltpu.VMEM(shape, dtype)
    dma = lambda *shape: pltpu.SemaphoreType.DMA(shape)
    state_msg = (STATE + 8, lanes)
    scratch = [
        vmem((tokens, width), BF16), vmem((width, lanes), BF16), vmem((tokens, STATE), BF16), vmem((tokens, STATE), BF16),
        vmem((2, tokens)), vmem((tokens, lanes), BF16), vmem((tokens, lanes), BF16),
        vmem((2 * blocks, BLK)), vmem((BLK, BLK)), vmem((blocks, lanes)),
        vmem((tokens, lanes)), vmem((tokens, 2 * BLK)), vmem((tokens, 2 * BLK)), vmem((tokens, lanes)),
        vmem((tokens, lanes)), vmem((tokens, lanes)), vmem((tokens, lanes)), vmem((tokens, lanes)), vmem((tokens, lanes)),
        vmem((blocks + 1, STATE, lanes)), vmem((blocks, STATE, lanes)), vmem((blocks, STATE, lanes)),
        vmem((STATE, lanes)), vmem((STATE, lanes)), vmem((lanes, tokens), BF16),
        vmem((2 * blocks, BLK)), vmem((2 * blocks, BLK)), vmem((blocks, lanes)),
        vmem(state_msg), vmem(state_msg), vmem((sp_count, *state_msg)), vmem((sp_count, *state_msg)),
        vmem((sp_count, lanes, cols)), vmem((8, HEAD, cols)), vmem((16, HEAD, cols)), vmem((8, HEAD, cols)),
        vmem((4, HEAD // 2, cols)), vmem((8, HEAD // 2, cols)),
        vmem((8, cols)), vmem((tp_count, 8, cols)),
        dma(6), dma(tokens // (2 * BLK)), dma(sp_count), dma(sp_count), dma(sp_count), dma(sp_count),
        dma(8), dma(8), dma(16), dma(16), dma(4), dma(4), dma(8), dma(8), dma(tp_count), dma(tp_count),
    ]
    hbm = pl.BlockSpec(memory_space=pl.ANY)
    in_vmem = pl.BlockSpec(memory_space=pltpu.VMEM)
    outs = pl.pallas_call(
        functools.partial(mixer, sp_count, tp_count),
        out_shape=(
            jax.ShapeDtypeStruct((tokens, STATE), F32),
            jax.ShapeDtypeStruct((tokens, STATE), F32),
            jax.ShapeDtypeStruct((2, tokens), F32),
            jax.ShapeDtypeStruct((tokens, lanes), F32),
            jax.ShapeDtypeStruct((cols, lanes), F32),
            jax.ShapeDtypeStruct((1, cols), F32),
        ),
        in_specs=[hbm, hbm, hbm, hbm, hbm, pl.BlockSpec(memory_space=pltpu.SMEM), hbm, hbm],
        out_specs=tuple([in_vmem] * 6),
        scratch_shapes=scratch,
        compiler_params=pltpu.CompilerParams(
            collective_id=0, has_side_effects=True, vmem_limit_bytes=60 * 1024 * 1024
        ),
        name="mixer",
    )(block_input, value_weight, key_rows, query_rows, decay_pre, decay_log, gate_rows, out_grad)
    return (*outs[:5], outs[5].reshape(cols))


def solution(mesh):
    in_specs = (
        P("sp", None),
        P(None, "tp"),
        P("sp", "tp"),
        P("sp", "tp"),
        P("tp", "sp"),
        P("tp"),
        P("sp", "tp"),
        P("sp", "tp"),
    )
    out_specs = (P("sp", "tp"), P("sp", "tp"), P("tp", "sp"), P("sp", "tp"), P("sp", "tp"), P("sp"))
    body = functools.partial(shards, mesh.shape["sp"], mesh.shape["tp"])
    return jax.shard_map(body, mesh=mesh, in_specs=in_specs, out_specs=out_specs, check_vma=False)
```

profile of v0, /device:TPU:1, one launch (start us, length us, event | category | flops | bytes accessed | tf_op | source)
XLA Modules:
  0.0 74.2 jit_solution(14646046054453292807)
XLA Ops:
  0.6 2.0 %copy.14.k_hbm = bf16[2048,64]{1,0:T(8,128)(2,1)} copy(bf16[2048,64]{0,1:T(8,128)(2,1)} %param.10) | data formatting | bytes 524288 | tf_op args[2]
  2.6 2.0 %copy.15.q_hbm = bf16[2048,64]{1,0:T(8,128)(2,1)} copy(bf16[2048,64]{0,1:T(8,128)(2,1)} %param.11) | data formatting | bytes 524288 | tf_op args[3]
  4.5 58.6 %mixer.1 = (f32[2048,64]{1,0:T(8,128)}, f32[2048,64]{1,0:T(8,128)}, f32[2,2048]{1,0:T(2,128)}, f32[2048,128]{1,0:T(8,128)}, f32[256,128]{1,0:T(8,128)}, /*index=5*/f32[1,256]{1,0:T(1,128)}) custom-call(bf16[2048,4096]{1,0:T(8,128)(2,1)} %x_hbm.1, bf16[4096,128]{1,0:T(8,128)(2,1)} %w_hbm.1, bf16[2048,64]{1,0:T(8,128)(2,1)} %copy.14.k_hbm, ...), custom_call_target="tpu_custom_call" | custom-call | tf_op jit(solution)/shard_map/mixer/pallas_call | solution.py:521
  63.2 2.3 %copy.16 = f32[2048,64]{0,1:T(8,128)} copy(f32[2048,64]{1,0:T(8,128)} %get-tuple-element.18) | data formatting | bytes 1048576
  65.5 2.3 %copy.17 = f32[2048,64]{0,1:T(8,128)} copy(f32[2048,64]{1,0:T(8,128)} %get-tuple-element.19) | data formatting | bytes 1048576
  67.9 1.3 %copy.22 = f32[2,2048]{1,0:T(2,128)} copy(f32[2,2048]{1,0:T(2,128)} %get-tuple-element.32) | data formatting | bytes 32768
  69.2 2.3 %copy.23 = f32[2048,128]{1,0:T(8,128)} copy(f32[2048,128]{1,0:T(8,128)} %get-tuple-element.33) | data formatting | bytes 2097152
  71.4 1.6 %copy.24 = f32[256,128]{1,0:T(8,128)} copy(f32[256,128]{1,0:T(8,128)} %get-tuple-element.34) | data formatting | bytes 262144
  73.0 1.2 %copy.25 = f32[256]{0:T(256)} copy(f32[256]{0:T(256)} %bitcast.1) | data formatting | bytes 2048
where the time goes:
time: 74.6 us; the launch traced here: 74.2 us
  Pallas kernels  58.6 us (79%)
  local copies, waits for them, and re-layouts  14.9 us (20%)
    pallas_call x1, Pallas kernels, shards(): pl.pallas_call(functools.partial(mixer, sp_count, tp_count), out_shape=(j...  58.6 us
    unnamed x8, local copies, waits for them, and re-layouts  14.9 us

commit v1 on v0

v1 whole, which is shorter than its diff:
```python
import functools

import jax
import jax.numpy as jnp
from jax import lax
from jax.experimental import pallas as pl
from jax.experimental.pallas import tpu as pltpu
from jax.sharding import PartitionSpec as P

HEAD = 64
STATE = 64
BLK = 128
RING = 4
F32 = jnp.float32
BF16 = jnp.bfloat16
HIGHEST = lax.Precision.HIGHEST
MESH = pl.DeviceIdType.MESH

ORDER = [
    [(2, 2)], [(2, 0), (0, 2)], [(2, 1), (1, 2)], [(2, 3), (3, 2)], [(1, 3), (3, 1)],
    [(3, 3), (1, 1)], [(1, 0), (0, 1)], [(3, 0), (0, 3)], [(0, 0)],
]


def nn(a, b, precision=None):
    return lax.dot_general(a, b, (((1,), (0,)), ((), ())), precision=precision, preferred_element_type=F32)


def nt(a, b, precision=None):
    return lax.dot_general(a, b, (((1,), (1,)), ((), ())), precision=precision, preferred_element_type=F32)


def tn(a, b, precision=None):
    return lax.dot_general(a, b, (((0,), (0,)), ((), ())), precision=precision, preferred_element_type=F32)


def halves(a):
    high = a.astype(BF16)
    return high, (a - high.astype(F32)).astype(BF16)


def both(a):
    return jnp.concatenate(halves(a), axis=1)


def folded(a):
    width = a.shape[1] // 2
    return a[:, :width] + a[:, width:]


def softplus(a):
    return jnp.maximum(a, 0.0) + jnp.log1p(jnp.exp(-jnp.abs(a)))


def sigmoid(a):
    return 1.0 / (1.0 + jnp.exp(-a))


def mixer(
    sp_count,
    tp_count,
    x_hbm, w_hbm, k_hbm, q_hbm, pre_hbm, rate_hbm, gate_hbm, cot_hbm,
    kg_ref, qg_ref, dg_ref, gg_ref, wg_ref, rn_ref,
    x_v, w_v, k_v, q_v, pre_v, rate_ref, gate_v, cot_v,
    rows_s, stack_s, rend_s,
    dy_s, tm_s, lm_s, er_s, te_s, se_s, p_s, v_s, u_s,
    gst_s, sst_s, bs_s, out_s, inc_s, vgt_s,
    yy_s, dd_s, ee_s,
    last_s, grow, gcol, srow, scol,
    part, far_r, near_r, red_s, far2_r, near2_r,
    nmsg, nslots,
    in_sem, x_sem, gs_sem, gr_sem, ss_sem, sr_sem, gs2_sem, gr2_sem, ss2_sem, sr2_sem,
    fs_sem, fr_sem, ns_sem, nr_sem, f2s_sem, f2r_sem, n2s_sem, n2r_sem, norm_s, norm_r,
):
    tokens, width = x_v.shape
    blocks = tokens // BLK
    lanes = 2 * HEAD
    cols = width // sp_count
    me = lax.axis_index("sp")
    my_tp = lax.axis_index("tp")
    mz, mx = lax.div(me, RING), lax.rem(me, RING)

    barrier = pltpu.get_barrier_semaphore()
    for off in range(1, RING):
        for peer in (mz * RING + lax.rem(mx + off, RING), lax.rem(mz + off, RING) * RING + mx):
            pl.semaphore_signal(barrier, inc=1, device_id={"sp": peer}, device_id_type=MESH)
    for off in range(1, tp_count):
        pl.semaphore_signal(
            barrier, inc=1, device_id={"tp": lax.rem(my_tp + off, tp_count)}, device_id_type=MESH
        )

    small = [
        pltpu.make_async_copy(src, dst, in_sem.at[i])
        for i, (src, dst) in enumerate(
            [
                (pre_hbm, pre_v), (rate_hbm, rate_ref), (gate_hbm, gate_v), (cot_hbm, cot_v), (q_hbm, q_v), (k_hbm, k_v), (w_hbm, w_v)
            ]
        )
    ]
    for copy in small:
        copy.start()
    xrows = tokens // x_sem.shape[0]
    xchunks = tokens // xrows

    def x_copy(i):
        rows = pl.ds(pl.multiple_of(i * xrows, xrows), xrows)
        return pltpu.make_async_copy(x_hbm.at[rows], x_v.at[rows], x_sem.at[i])

    small[0].wait()
    small[1].wait()
    for h in range(2):
        for c in range(blocks):
            rows_s[h * blocks + c : h * blocks + c + 1, :] = pre_v[h : h + 1, c * BLK : (c + 1) * BLK]
    pre = rows_s[...]
    row_id = lax.broadcasted_iota(jnp.int32, (2 * blocks, BLK), 0)
    rate = jnp.where(
        row_id < blocks,
        jnp.exp(jnp.full((2 * blocks, BLK), rate_ref[0], F32)),
        jnp.exp(jnp.full((2 * blocks, BLK), rate_ref[1], F32)),
    )
    step = softplus(pre)
    sq_row = lax.broadcasted_iota(jnp.int32, (BLK, BLK), 0)
    sq_col = lax.broadcasted_iota(jnp.int32, (BLK, BLK), 1)
    lower = sq_row >= sq_col
    run = nn(-rate * step, (sq_row <= sq_col).astype(F32), HIGHEST)
    stack_s[...] = jnp.zeros_like(stack_s)
    stack_s[0 : 2 * blocks, :] = run
    stack_s[2 * blocks : 4 * blocks, :] = step
    turned = stack_s[...].T
    first_head = lax.broadcasted_iota(jnp.int32, (BLK, lanes), 1) < HEAD
    for copy in small[2:6]:
        copy.wait()
    for i in range(xchunks):
        x_copy(i).start()

    def block_rows(c):
        return pl.ds(pl.multiple_of(c * BLK, BLK), BLK)

    def for_blocks(start, stop, unroll, body):
        def step_of(i, carry):
            for b in range(unroll):
                body(start + i * unroll + b)
            return carry

        lax.fori_loop(0, (stop - start) // unroll, step_of, 0)

    def columns_of(c, kinds):
        rolled = pltpu.roll(turned, lax.rem(BLK - c, BLK), 1)
        return [jnp.broadcast_to(rolled[:, i * blocks : i * blocks + 1], (BLK, BLK)) for i in kinds]

    def prepare(c):
        rows = block_rows(c)
        running = jnp.where(first_head, *columns_of(c, (0, 1)))
        er = jnp.exp(running)
        er_s[rows, :] = er
        rend_s[pl.ds(c, 1), :] = running[BLK - 1 : BLK, :]
        gate = gate_v[rows, :].astype(F32)
        dy = cot_v[rows, :].astype(F32) * gate * sigmoid(gate)
        dy_s[rows, :] = dy
        bs_s[c] = folded(nn(q_v[:, rows], both(er * dy)))

    for_blocks(0, blocks, min(4, blocks), prepare)
    grad = jnp.zeros((STATE, lanes), F32)
    total = jnp.zeros((1, lanes), F32)
    for c in reversed(range(blocks)):
        end = rend_s[c : c + 1, :]
        grad = jnp.exp(end) * grad + bs_s[c]
        total = total + end
        gst_s[c] = grad
    def message(ref, at, value, log):
        ref[at, 0:STATE, :] = value
        ref[at, STATE : STATE + 8, :] = jnp.broadcast_to(log, (8, lanes))

    def row_copy(slots, send, recv, source, target):
        return pltpu.make_async_remote_copy(
            src_ref=slots.at[source],
            dst_ref=slots.at[source],
            send_sem=send.at[target],
            recv_sem=recv.at[source],
            device_id={"sp": mz * RING + target},
            device_id_type=MESH,
        )

    def col_copy(slots, send, recv, source, target):
        return pltpu.make_async_remote_copy(
            src_ref=slots.at[source],
            dst_ref=slots.at[source],
            send_sem=send.at[target],
            recv_sem=recv.at[source],
            device_id={"sp": target * RING + mx},
            device_id_type=MESH,
        )

    def send_row(slots, send, recv):
        for off in range(1, RING):
            row_copy(slots, send, recv, mx, lax.rem(mx + off, RING)).start()

    def row_sum(slots, send, recv, order):
        for off in range(1, RING):
            row_copy(slots, send, recv, lax.rem(mx + off, RING), mx).wait_recv()
        acc = jnp.zeros((STATE, lanes), F32)
        log = jnp.zeros((1, lanes), F32)
        own, own_log = acc, log
        for at in order:
            own = jnp.where(mx == at, acc, own)
            own_log = jnp.where(mx == at, log, own_log)
            tail = slots[at, STATE : STATE + 1, :]
            acc = slots[at, 0:STATE, :] + jnp.exp(tail) * acc
            log = log + tail
        return own, own_log, acc, log

    message(grow, mx, grad, total)
    pl.semaphore_wait(barrier, 2 * (RING - 1) + tp_count - 1)
    send_row(grow, gs_sem, gr_sem)

    def project(i):
        x_copy(i).wait()
        rows = pl.ds(pl.multiple_of(i * xrows, xrows), xrows)
        p_s[rows, :] = nn(x_v[rows, :], w_v[...]).astype(BF16).astype(F32)

    def local(c):
        rows = block_rows(c)
        col = columns_of(c, range(4))
        scores = tn(q_v[:, rows], k_v[:, rows])
        weights = []
        for h in range(2):
            row = stack_s[pl.ds(h * blocks + c, 1), :]
            decay = jnp.exp(jnp.where(lower, col[h] - row, -1e30))
            lm_s[rows, h * BLK : (h + 1) * BLK] = decay
            weights.append(scores * decay)
        weights = jnp.concatenate(weights, axis=1)
        tm_s[rows, :] = weights
        running = jnp.where(first_head, col[0], col[1])
        te_s[rows, :] = jnp.exp(running[BLK - 1 : BLK, :] - running)
        se_s[rows, :] = jnp.where(first_head, col[2], col[3])
        dy_high, dy_low = halves(dy_s[rows, :])
        t_high, t_low = halves(weights)
        u = folded(tn(t_high, jnp.concatenate([dy_high, dy_low], axis=1))) + tn(t_low, dy_high)
        u_s[rows, :] = jnp.where(first_head, u[0:BLK, :], u[BLK : 2 * BLK, :])

    def with_values(c):
        rows = block_rows(c)
        projected = p_s[rows, :]
        v = projected * sigmoid(projected)
        v_s[rows, :] = v
        bs_s[c] = folded(nn(k_v[:, rows], both(te_s[rows, :] * se_s[rows, :] * v)))

    for_blocks(0, blocks, min(4, blocks), local)
    small[6].wait()

    def chunk(i, carry):
        project(i)
        return carry

    lax.fori_loop(0, xchunks // 2, chunk, 0)
    own_grad, own_log, ring_grad, ring_log = row_sum(grow, gs_sem, gr_sem, (3, 2, 1, 0))
    message(gcol, mz, ring_grad, ring_log)
    for target in range(RING - 1):

        @pl.when(target < mz)
        def _(target=target):
            col_copy(gcol, gs2_sem, gr2_sem, mz, target).start()

    lax.fori_loop(xchunks // 2, xchunks, chunk, 0)
    for_blocks(0, blocks, min(4, blocks), with_values)
    state = jnp.zeros((STATE, lanes), F32)
    for c in range(blocks):
        sst_s[c] = state
        state = jnp.exp(rend_s[c : c + 1, :]) * state + bs_s[c]
    last_s[...] = state
    message(srow, mx, state, total)
    send_row(srow, ss_sem, sr_sem)

    out_s[...] = jnp.zeros_like(out_s)
    for source in reversed(range(1, RING)):

        @pl.when(source > mz)
        def _(source=source):
            col_copy(gcol, gs2_sem, gr2_sem, source, mz).wait_recv()
            out_s[...] = gcol[source, 0:STATE, :] + jnp.exp(gcol[source, STATE : STATE + 1, :]) * out_s[...]

    out_s[...] = own_grad + jnp.exp(own_log) * out_s[...]
    after = jnp.zeros((1, lanes), F32)
    for c in reversed(range(blocks)):
        after = after + rend_s[c : c + 1, :]
        gst_s[c] = gst_s[c] + jnp.exp(after) * out_s[...]
    gst_s[blocks] = out_s[...]

    def value_gradient(c):
        rows = block_rows(c)
        u = u_s[rows, :] + te_s[rows, :] * folded(tn(k_v[:, rows], both(gst_s[c + 1])))
        u_s[rows, :] = u
        projected = p_s[rows, :]
        sig = sigmoid(projected)
        vg = se_s[rows, :] * u * sig * (1.0 + projected * (1.0 - sig))
        vgt_s[:, rows] = vg.astype(BF16).T

    for_blocks(0, blocks, min(4, blocks), value_gradient)

    def owner(dz, dx):
        return lax.rem(mz + dz, RING) * RING + lax.rem(mx + dx, RING)

    def neighbour(half, stage, direction):
        if half == stage:
            return lax.rem(mz + direction + RING, RING) * RING + mx
        return mz * RING + lax.rem(mx + direction + RING, RING)

    def half_of(half, dz, dx):
        return part.at[owner(dz, dx), half * HEAD : (half + 1) * HEAD, :]

    def piece(half, dist, across):
        return half_of(half, dist, across) if half == 0 else half_of(half, across, dist)

    def far_copy(half, across):
        direction = 1 if across < 2 else -1
        slot = half * RING + across
        return pltpu.make_async_remote_copy(
            src_ref=piece(half, 2, across),
            dst_ref=far_r.at[slot],
            send_sem=fs_sem.at[slot],
            recv_sem=fr_sem.at[slot],
            device_id={"sp": neighbour(half, 0, direction)},
            device_id_type=MESH,
        )

    def near_copy(half, direction, across):
        slot = (half * 2 + (0 if direction == 1 else 1)) * RING + across
        return pltpu.make_async_remote_copy(
            src_ref=piece(half, 1 if direction == 1 else 3, across),
            dst_ref=near_r.at[slot],
            send_sem=ns_sem.at[slot],
            recv_sem=nr_sem.at[slot],
            device_id={"sp": neighbour(half, 0, direction)},
            device_id_type=MESH,
        )

    for number, group in enumerate(ORDER):
        if number == 4:
            own_state, own_state_log, ring_state, ring_log = row_sum(srow, ss_sem, sr_sem, (0, 1, 2, 3))
            message(scol, mz, ring_state, ring_log)
            for target in range(1, RING):

                @pl.when(target > mz)
                def _(target=target):
                    col_copy(scol, ss2_sem, sr2_sem, mz, target).start()
        for dz, dx in group:
            dest = owner(dz, dx)
            columns = pl.ds(pl.multiple_of(dest * cols, cols), cols)
            part[dest] = nn(vgt_s[...], x_v[:, columns])
        for dz, dx in group:
            for half, dist, across in ((0, dz, dx), (1, dx, dz)):
                if dist == 2:
                    far_copy(half, across).start()
                elif dist == 1 and across >= 2:
                    near_copy(half, 1, across).start()
                elif dist == 3 and across < 2:
                    near_copy(half, -1, across).start()
    for across in range(2):
        for half in range(2):
            for direction, lane in ((1, across), (-1, across + 2)):
                far_copy(half, lane).wait_recv()
                ref = piece(half, 1 if direction == 1 else 3, lane)
                ref[...] = ref[...] + far_r[half * RING + lane]
                near_copy(half, direction, lane).start()

    inc_s[...] = jnp.zeros_like(inc_s)
    for source in range(RING - 1):

        @pl.when(source < mz)
        def _(source=source):
            col_copy(scol, ss2_sem, sr2_sem, source, mz).wait_recv()
            inc_s[...] = scol[source, 0:STATE, :] + jnp.exp(scol[source, STATE : STATE + 1, :]) * inc_s[...]

    inc_s[...] = own_state + jnp.exp(own_state_log) * inc_s[...]
    before = jnp.zeros((1, lanes), F32)
    for c in range(blocks):
        full = sst_s[c] + jnp.exp(before) * inc_s[...]
        sst_s[c] = full
        before = before + rend_s[c : c + 1, :]
        if c > 0:
            ee_s[c - 1 : c, :] = jnp.sum(full * gst_s[c], axis=0, keepdims=True)
    last = last_s[...] + jnp.exp(before) * inc_s[...]
    ee_s[blocks - 1 : blocks, :] = jnp.sum(last * gst_s[blocks], axis=0, keepdims=True)

    zero = jnp.zeros((BLK, lanes), BF16)
    lane_id = lax.broadcasted_iota(jnp.int32, (BLK, lanes), 1)
    yy_s[...] = jnp.zeros_like(yy_s)
    dd_s[...] = jnp.zeros_like(dd_s)

    def keep_head_sums(ref, c, a):
        first = jnp.sum(jnp.where(first_head, a, 0.0), axis=1, keepdims=True)
        second = jnp.sum(jnp.where(first_head, 0.0, a), axis=1, keepdims=True)
        ref[...] = jnp.where(lane_id == c, first, jnp.where(lane_id == blocks + c, second, ref[...]))

    def others(c):
        rows = block_rows(c)
        q, k = q_v[:, rows], k_v[:, rows]
        dy, v, u, er, te = dy_s[rows, :], v_s[rows, :], u_s[rows, :], er_s[rows, :], te_s[rows, :]
        sv = se_s[rows, :] * v
        sv_high, sv_low = halves(sv)

        def split_heads(a, axis):
            return jnp.concatenate([jnp.where(first_head, a, zero), jnp.where(first_head, zero, a)], axis=axis)

        spread = jnp.concatenate([split_heads(sv_high, 0), split_heads(sv_low, 0)], axis=1)
        mixed = folded(nn(tm_s[rows, :].astype(BF16), spread)) + er * folded(tn(q, both(sst_s[c])))
        gate = gate_v[rows, :].astype(F32)
        sig = sigmoid(gate)
        gg_ref[rows, :] = cot_v[rows, :].astype(F32) * mixed * sig * (1.0 + gate * (1.0 - sig))
        dp = nt(split_heads(dy.astype(BF16), 0), sv_high)
        d = dp[0:BLK, :] * lm_s[rows, 0:BLK] + dp[BLK : 2 * BLK, :] * lm_s[rows, BLK : 2 * BLK]
        d_high, d_low = halves(d)
        qg_ref[:, rows] = nt(
            jnp.concatenate([k, k], axis=1), jnp.concatenate([d_high, d_low], axis=1)
        ) + nt(sst_s[c].astype(BF16), (er * dy).astype(BF16))
        kg_ref[:, rows] = nn(
            jnp.concatenate([q, q], axis=1), jnp.concatenate([d_high, d_low], axis=0)
        ) + nt(gst_s[c + 1].astype(BF16), (te * sv).astype(BF16))
        keep_head_sums(yy_s, c, dy * mixed)
        keep_head_sums(dd_s, c, v * u)

    for_blocks(0, blocks, 2, others)
    ends = ee_s[...]
    end_cols = jnp.concatenate(
        [
            jnp.sum(ends[:, 0:HEAD], axis=1, keepdims=True),
            jnp.sum(ends[:, HEAD:lanes], axis=1, keepdims=True),
        ],
        axis=0,
    )
    direct = dd_s[...].T[0 : 2 * blocks, :]
    log_grad = nn(yy_s[...].T[0 : 2 * blocks, :] - step * direct, lower.astype(F32), HIGHEST) + end_cols
    decay_grad = (direct - rate * log_grad) * sigmoid(pre)
    for h in range(2):
        for c in range(blocks):
            dg_ref[h : h + 1, c * BLK : (c + 1) * BLK] = decay_grad[h * blocks + c : h * blocks + c + 1, :]

    quarter = HEAD // 2

    def total_of(half, across):
        plus, minus = (half * 2) * RING + across, (half * 2 + 1) * RING + across
        near_copy(half, 1, across).wait_recv()
        near_copy(half, -1, across).wait_recv()
        return piece(half, 0, across)[...] + near_r[plus] + near_r[minus]

    def far2_copy(half, which):
        slot = half * 2 + which
        return pltpu.make_async_remote_copy(
            src_ref=red_s.at[half * RING + 2, which * quarter : (which + 1) * quarter, :],
            dst_ref=far2_r.at[slot],
            send_sem=f2s_sem.at[slot],
            recv_sem=f2r_sem.at[slot],
            device_id={"sp": neighbour(half, 1, 1 if which == 0 else -1)},
            device_id_type=MESH,
        )

    def near2_copy(half, direction, which):
        side = 0 if direction == 1 else 1
        slot = (half * 2 + side) * 2 + which
        return pltpu.make_async_remote_copy(
            src_ref=red_s.at[half * RING + (1 if direction == 1 else 3), which * quarter : (which + 1) * quarter, :],
            dst_ref=near2_r.at[slot],
            send_sem=n2s_sem.at[slot],
            recv_sem=n2r_sem.at[slot],
            device_id={"sp": neighbour(half, 1, direction)},
            device_id_type=MESH,
        )

    for across in (2, 1, 3, 0):
        for half in range(2):
            red_s[half * RING + across] = total_of(half, across)
            if across == 2:
                far2_copy(half, 0).start()
                far2_copy(half, 1).start()
            elif across == 1:
                near2_copy(half, 1, 1).start()
            elif across == 3:
                near2_copy(half, -1, 0).start()
    for half in range(2):
        for direction, which in ((1, 0), (-1, 1)):
            far2_copy(half, which).wait_recv()
            at = half * RING + (1 if direction == 1 else 3)
            span = slice(which * quarter, (which + 1) * quarter)
            red_s[at, span, :] = red_s[at, span, :] + far2_r[half * 2 + which]
            near2_copy(half, direction, which).start()

    squares = jnp.zeros((1, cols), F32)
    for half in range(2):
        for which in range(2):
            for direction in (1, -1):
                near2_copy(half, direction, which).wait_recv()
            plus, minus = (half * 2) * 2 + which, (half * 2 + 1) * 2 + which
            span = slice(which * quarter, (which + 1) * quarter)
            done = red_s[half * RING, span, :] + near2_r[plus] + near2_r[minus]
            red_s[half * RING, span, :] = done
            squares = squares + jnp.sum(done * done, axis=0, keepdims=True)

    def norm_copy(source, target):
        return pltpu.make_async_remote_copy(
            src_ref=nmsg,
            dst_ref=nslots.at[source],
            send_sem=norm_s.at[target],
            recv_sem=norm_r.at[source],
            device_id={"tp": target},
            device_id_type=MESH,
        )

    nmsg[...] = jnp.broadcast_to(squares, (8, cols))
    for off in range(1, tp_count):
        norm_copy(my_tp, lax.rem(my_tp + off, tp_count)).start()
    for half in range(2):
        wg_ref[:, half * HEAD : (half + 1) * HEAD] = red_s[half * RING].T
    norms = squares
    for off in range(1, tp_count):
        source = lax.rem(my_tp + off, tp_count)
        norm_copy(source, my_tp).wait_recv()
        norms = norms + nslots[source, 0:1, :]
    rn_ref[...] = norms

    for off in range(1, RING):
        row_copy(grow, gs_sem, gr_sem, mx, lax.rem(mx + off, RING)).wait_send()
        row_copy(srow, ss_sem, sr_sem, mx, lax.rem(mx + off, RING)).wait_send()
    for target in range(RING):

        @pl.when(target < mz)
        def _(target=target):
            col_copy(gcol, gs2_sem, gr2_sem, mz, target).wait_send()

        @pl.when(target > mz)
        def _(target=target):
            col_copy(scol, ss2_sem, sr2_sem, mz, target).wait_send()

    for half in range(2):
        for across in range(RING):
            far_copy(half, across).wait_send()
            for direction in (1, -1):
                near_copy(half, direction, across).wait_send()
        for which in range(2):
            far2_copy(half, which).wait_send()
            for direction in (1, -1):
                near2_copy(half, direction, which).wait_send()
    for off in range(1, tp_count):
        norm_copy(my_tp, lax.rem(my_tp + off, tp_count)).wait_send()


def put_out(*refs):
    sources, targets, sems = refs[:6], refs[6:12], refs[12]
    copies = [pltpu.make_async_copy(s, t, sems.at[i]) for i, (s, t) in enumerate(zip(sources, targets))]
    for copy in copies:
        copy.start()
    for copy in copies:
        copy.wait()


def shards(sp_count, tp_count, block_input, value_weight, key_rows, query_rows, decay_pre, decay_log, gate_rows, out_grad):
    tokens, width = block_input.shape
    blocks = tokens // BLK
    lanes = 2 * HEAD
    cols = width // sp_count
    vmem = lambda shape, dtype=F32: pltpu.VMEM(shape, dtype)
    dma = lambda *shape: pltpu.SemaphoreType.DMA(shape)
    state_msg = (STATE + 8, lanes)
    scratch = [
        vmem((tokens, width), BF16), vmem((width, lanes), BF16), vmem((STATE, tokens), BF16), vmem((STATE, tokens), BF16),
        vmem((2, tokens)), pltpu.SMEM((2,), F32), vmem((tokens, lanes), BF16), vmem((tokens, lanes), BF16),
        vmem((2 * blocks, BLK)), vmem((BLK, BLK)), vmem((blocks, lanes)),
        vmem((tokens, lanes)), vmem((tokens, 2 * BLK)), vmem((tokens, 2 * BLK)), vmem((tokens, lanes)),
        vmem((tokens, lanes)), vmem((tokens, lanes)), vmem((tokens, lanes)), vmem((tokens, lanes)), vmem((tokens, lanes)),
        vmem((blocks + 1, STATE, lanes)), vmem((blocks, STATE, lanes)), vmem((blocks, STATE, lanes)),
        vmem((STATE, lanes)), vmem((STATE, lanes)), vmem((lanes, tokens), BF16),
        vmem((BLK, lanes)), vmem((BLK, lanes)), vmem((blocks, lanes)),
        vmem((STATE, lanes)), *(vmem((RING, *state_msg)) for _ in range(4)),
        vmem((sp_count, lanes, cols)), vmem((8, HEAD, cols)), vmem((16, HEAD, cols)), vmem((8, HEAD, cols)),
        vmem((4, HEAD // 2, cols)), vmem((8, HEAD // 2, cols)),
        vmem((8, cols)), vmem((tp_count, 8, cols)),
        dma(7), dma(max(2, tokens // (4 * BLK))), *(dma(RING) for _ in range(8)),
        dma(8), dma(8), dma(16), dma(16), dma(4), dma(4), dma(8), dma(8), dma(tp_count), dma(tp_count),
    ]
    hbm = pl.BlockSpec(memory_space=pltpu.HBM)
    in_vmem = pl.BlockSpec(memory_space=pltpu.VMEM)
    outs = pl.pallas_call(
        functools.partial(mixer, sp_count, tp_count),
        out_shape=(
            jax.ShapeDtypeStruct((STATE, tokens), F32),
            jax.ShapeDtypeStruct((STATE, tokens), F32),
            jax.ShapeDtypeStruct((2, tokens), F32),
            jax.ShapeDtypeStruct((tokens, lanes), F32),
            jax.ShapeDtypeStruct((cols, lanes), F32),
            jax.ShapeDtypeStruct((1, cols), F32),
        ),
        in_specs=[hbm] * 8,
        out_specs=tuple([in_vmem] * 6),
        scratch_shapes=scratch,
        compiler_params=pltpu.CompilerParams(
            collective_id=0, has_side_effects=True, vmem_limit_bytes=46 * 1024 * 1024
        ),
        name="mixer",
    )(
        *(pltpu.with_memory_space_constraint(a, pltpu.HBM) for a in (block_input, value_weight, key_rows.T, query_rows.T, decay_pre)),
        pltpu.with_memory_space_constraint(decay_log, pltpu.HBM),
        *(pltpu.with_memory_space_constraint(a, pltpu.HBM) for a in (gate_rows, out_grad)),
    )
    kg, qg, dg, gg, wg, rn = pl.pallas_call(
        put_out,
        out_shape=tuple(jax.ShapeDtypeStruct(o.shape, o.dtype) for o in outs),
        in_specs=[in_vmem] * 6,
        out_specs=tuple([hbm] * 6),
        scratch_shapes=[dma(6)],
        compiler_params=pltpu.CompilerParams(vmem_limit_bytes=8 * 1024 * 1024),
        name="put_out",
    )(*outs)
    return kg.T, qg.T, dg, gg, wg, rn.reshape(cols)


def solution(mesh):
    in_specs = (
        P("sp", None),
        P(None, "tp"),
        P("sp", "tp"),
        P("sp", "tp"),
        P("tp", "sp"),
        P("tp"),
        P("sp", "tp"),
        P("sp", "tp"),
    )
    out_specs = (P("sp", "tp"), P("sp", "tp"), P("tp", "sp"), P("sp", "tp"), P("sp", "tp"), P("sp"))
    body = functools.partial(shards, mesh.shape["sp"], mesh.shape["tp"])
    return jax.shard_map(body, mesh=mesh, in_specs=in_specs, out_specs=out_specs, check_vma=False)
```

time: 74.6 us -> 49.3 us (0.66)
  local copies, waits for them, and re-layouts: 14.9 us -> 0 us
  Pallas kernels: 58.6 us -> 48.5 us
    unnamed x8 -> x0, local copies, waits for them, and re-layouts: 14.9 us -> none
    pallas_call x1, Pallas kernels: 58.6 us -> 47.1 us  [shards(): pl.pallas_call(functools.partial(mixer, sp_count, tp_count), out_shape=(j...]
    pallas_call x0 -> x1, Pallas kernels: none -> 1.41 us  [shards(): pl.pallas_call(put_out, out_shape=tuple((jax.ShapeDtypeStruct(o.shape, o....]
where the time goes in v1:
time: 49.3 us; the launch traced here: 49.2 us
  Pallas kernels  48.5 us (98%)
  between operations  0.64 us (1%)
    pallas_call x1, Pallas kernels, shards(): pl.pallas_call(functools.partial(mixer, sp_count, tp_count), out_shape=(j...  47.1 us
    pallas_call x1, Pallas kernels, shards(): pl.pallas_call(put_out, out_shape=tuple((jax.ShapeDtypeStruct(o.shape, o....  1.41 us

profile of v1, /device:TPU:1, one launch (start us, length us, event | category | flops | bytes accessed | tf_op | source)
XLA Modules:
  0.0 49.2 jit_solution(12919761040649746215)
XLA Ops:
  0.6 47.1 %mixer.1 = (f32[64,2048]{1,0:T(8,128)S(1)}, f32[64,2048]{1,0:T(8,128)S(1)}, f32[2,2048]{1,0:T(2,128)S(1)}, f32[2048,128]{1,0:T(8,128)S(1)}, f32[256,128]{1,0:T(8,128)S(1)}, /*index=5*/f32[1,256]{1,0:T(1,128)S(1)}) custom-call(bf16[2048,4096]{1,0:T(8,128)(2,1)} %x_hbm.1, bf16[4096,128]{1,0:T(8,128)(2,1)} %w_hbm.1, bf16[64,2048]{1,0:T(8,128)(2,1)} %bitcast.5, ...), custom_call_target="tpu_custom_call" | custom-call | tf_op jit(solution)/shard_map/mixer/pallas_call | solution.py:581
  47.7 1.4 %put_out.1 = (f32[64,2048]{1,0:T(8,128)}, f32[64,2048]{1,0:T(8,128)}, f32[2,2048]{1,0:T(2,128)}, f32[2048,128]{1,0:T(8,128)}, f32[256,128]{1,0:T(8,128)}, /*index=5*/f32[1,256]{1,0:T(1,128)}) custom-call(f32[64,2048]{1,0:T(8,128)S(1)} %get-tuple-element.18.refs_0_, f32[64,2048]{1,0:T(8,128)S(1)} %get-tuple-element.19.refs_1_, ...), custom_call_target="tpu_custom_call" | custom-call | tf_op jit(solution)/shard_map/put_out/pallas_call | solution.py:603

commit v2 on v1

--- a/solution.py
+++ b/solution.py
@@ -61,6 +61,7 @@
     tp_count,
     x_hbm, w_hbm, k_hbm, q_hbm, pre_hbm, rate_hbm, gate_hbm, cot_hbm,
     kg_ref, qg_ref, dg_ref, gg_ref, wg_ref, rn_ref,
+    m_s,
     x_v, w_v, k_v, q_v, pre_v, rate_ref, gate_v, cot_v,
     rows_s, stack_s, rend_s,
     dy_s, tm_s, lm_s, er_s, te_s, se_s, p_s, v_s, u_s,
@@ -97,7 +98,7 @@
             ]
         )
     ]
-    for copy in small:
+    for copy in small[:6]:
         copy.start()
     xrows = tokens // x_sem.shape[0]
     xchunks = tokens // xrows
@@ -121,6 +122,7 @@
     step = softplus(pre)
     sq_row = lax.broadcasted_iota(jnp.int32, (BLK, BLK), 0)
     sq_col = lax.broadcasted_iota(jnp.int32, (BLK, BLK), 1)
+    upper = sq_row <= sq_col
     lower = sq_row >= sq_col
     run = nn(-rate * step, (sq_row <= sq_col).astype(F32), HIGHEST)
     stack_s[...] = jnp.zeros_like(stack_s)
@@ -130,6 +132,7 @@
     first_head = lax.broadcasted_iota(jnp.int32, (BLK, lanes), 1) < HEAD
     for copy in small[2:6]:
         copy.wait()
+    small[6].start()
     for i in range(xchunks):
         x_copy(i).start()
 
@@ -159,7 +162,7 @@
         dy_s[rows, :] = dy
         bs_s[c] = folded(nn(q_v[:, rows], both(er * dy)))
 
-    for_blocks(0, blocks, min(4, blocks), prepare)
+    for_blocks(0, blocks, min(8, blocks), prepare)
     grad = jnp.zeros((STATE, lanes), F32)
     total = jnp.zeros((1, lanes), F32)
     for c in reversed(range(blocks)):
@@ -171,13 +174,23 @@
         ref[at, 0:STATE, :] = value
         ref[at, STATE : STATE + 8, :] = jnp.broadcast_to(log, (8, lanes))
 
-    def row_copy(slots, send, recv, source, target):
-        return pltpu.make_async_remote_copy(
-            src_ref=slots.at[source],
-            dst_ref=slots.at[source],
-            send_sem=send.at[target],
-            recv_sem=recv.at[source],
+    def row_copy(slots, send, recv, target):
+        return pltpu.make_async_remote_copy(
+            src_ref=slots.at[mx],
+            dst_ref=slots.at[mx],
+            send_sem=send.at[0],
+            recv_sem=recv.at[0],
             device_id={"sp": mz * RING + target},
+            device_id_type=MESH,
+        )
+
+    def all_of(refs, send, recv):
+        return pltpu.make_async_remote_copy(
+            src_ref=refs,
+            dst_ref=refs,
+            send_sem=send,
+            recv_sem=recv,
+            device_id={"sp": mz * RING + lax.rem(mx + 1, RING)},
             device_id_type=MESH,
         )
 
@@ -192,12 +205,11 @@
         )
 
     def send_row(slots, send, recv):
-        for off in range(1, RING):
-            row_copy(slots, send, recv, mx, lax.rem(mx + off, RING)).start()
+        for off in (2, 1, 3):
+            row_copy(slots, send, recv, lax.rem(mx + off, RING)).start()
 
     def row_sum(slots, send, recv, order):
-        for off in range(1, RING):
-            row_copy(slots, send, recv, lax.rem(mx + off, RING), mx).wait_recv()
+        all_of(slots.at[0 : RING - 1], send.at[0], recv.at[0]).wait_recv()
         acc = jnp.zeros((STATE, lanes), F32)
         log = jnp.zeros((1, lanes), F32)
         own, own_log = acc, log
@@ -221,21 +233,23 @@
     def local(c):
         rows = block_rows(c)
         col = columns_of(c, range(4))
-        scores = tn(q_v[:, rows], k_v[:, rows])
-        weights = []
-        for h in range(2):
-            row = stack_s[pl.ds(h * blocks + c, 1), :]
-            decay = jnp.exp(jnp.where(lower, col[h] - row, -1e30))
-            lm_s[rows, h * BLK : (h + 1) * BLK] = decay
-            weights.append(scores * decay)
-        weights = jnp.concatenate(weights, axis=1)
-        tm_s[rows, :] = weights
+        pair = pl.ds(pl.multiple_of(c * 2 * BLK, 2 * BLK), 2 * BLK)
+        scores = tn(k_v[:, rows], q_v[:, rows])
+        decay = jnp.concatenate(
+            [
+                jnp.exp(jnp.where(upper, stack_s[pl.ds(h * blocks + c, 1), :] - col[h], -1e30))
+                for h in range(2)
+            ],
+            axis=0,
+        )
+        lm_s[pair, :] = decay
         running = jnp.where(first_head, col[0], col[1])
         te_s[rows, :] = jnp.exp(running[BLK - 1 : BLK, :] - running)
         se_s[rows, :] = jnp.where(first_head, col[2], col[3])
         dy_high, dy_low = halves(dy_s[rows, :])
-        t_high, t_low = halves(weights)
-        u = folded(tn(t_high, jnp.concatenate([dy_high, dy_low], axis=1))) + tn(t_low, dy_high)
+        t_high, t_low = halves(jnp.concatenate([scores, scores], axis=0) * decay)
+        tm_s[pair, :] = t_high
+        u = folded(nn(t_high, jnp.concatenate([dy_high, dy_low], axis=1))) + nn(t_low, dy_high)
         u_s[rows, :] = jnp.where(first_head, u[0:BLK, :], u[BLK : 2 * BLK, :])
 
     def with_values(c):
@@ -252,16 +266,15 @@
         project(i)
         return carry
 
-    lax.fori_loop(0, xchunks // 2, chunk, 0)
     own_grad, own_log, ring_grad, ring_log = row_sum(grow, gs_sem, gr_sem, (3, 2, 1, 0))
     message(gcol, mz, ring_grad, ring_log)
-    for target in range(RING - 1):
+    for target in (1, 0, 2):
 
         @pl.when(target < mz)
         def _(target=target):
             col_copy(gcol, gs2_sem, gr2_sem, mz, target).start()
 
-    lax.fori_loop(xchunks // 2, xchunks, chunk, 0)
+    lax.fori_loop(0, xchunks, chunk, 0)
     for_blocks(0, blocks, min(4, blocks), with_values)
     state = jnp.zeros((STATE, lanes), F32)
     for c in range(blocks):
@@ -317,32 +330,24 @@
         return pltpu.make_async_remote_copy(
             src_ref=piece(half, 2, across),
             dst_ref=far_r.at[slot],
-            send_sem=fs_sem.at[slot],
+            send_sem=fs_sem.at[0],
             recv_sem=fr_sem.at[slot],
             device_id={"sp": neighbour(half, 0, direction)},
             device_id_type=MESH,
         )
 
     def near_copy(half, direction, across):
-        slot = (half * 2 + (0 if direction == 1 else 1)) * RING + across
+        pair = half * RING + across
         return pltpu.make_async_remote_copy(
             src_ref=piece(half, 1 if direction == 1 else 3, across),
-            dst_ref=near_r.at[slot],
-            send_sem=ns_sem.at[slot],
-            recv_sem=nr_sem.at[slot],
+            dst_ref=near_r.at[2 * pair + (0 if direction == 1 else 1)],
+            send_sem=ns_sem.at[0],
+            recv_sem=nr_sem.at[pair],
             device_id={"sp": neighbour(half, 0, direction)},
             device_id_type=MESH,
         )
 
-    for number, group in enumerate(ORDER):
-        if number == 4:
-            own_state, own_state_log, ring_state, ring_log = row_sum(srow, ss_sem, sr_sem, (0, 1, 2, 3))
-            message(scol, mz, ring_state, ring_log)
-            for target in range(1, RING):
-
-                @pl.when(target > mz)
-                def _(target=target):
-                    col_copy(scol, ss2_sem, sr2_sem, mz, target).start()
+    for group in ORDER:
         for dz, dx in group:
             dest = owner(dz, dx)
             columns = pl.ds(pl.multiple_of(dest * cols, cols), cols)
@@ -355,33 +360,6 @@
                     near_copy(half, 1, across).start()
                 elif dist == 3 and across < 2:
                     near_copy(half, -1, across).start()
-    for across in range(2):
-        for half in range(2):
-            for direction, lane in ((1, across), (-1, across + 2)):
-                far_copy(half, lane).wait_recv()
-                ref = piece(half, 1 if direction == 1 else 3, lane)
-                ref[...] = ref[...] + far_r[half * RING + lane]
-                near_copy(half, direction, lane).start()
-
-    inc_s[...] = jnp.zeros_like(inc_s)
-    for source in range(RING - 1):
-
-        @pl.when(source < mz)
-        def _(source=source):
-            col_copy(scol, ss2_sem, sr2_sem, source, mz).wait_recv()
-            inc_s[...] = scol[source, 0:STATE, :] + jnp.exp(scol[source, STATE : STATE + 1, :]) * inc_s[...]
-
-    inc_s[...] = own_state + jnp.exp(own_state_log) * inc_s[...]
-    before = jnp.zeros((1, lanes), F32)
-    for c in range(blocks):
-        full = sst_s[c] + jnp.exp(before) * inc_s[...]
-        sst_s[c] = full
-        before = before + rend_s[c : c + 1, :]
-        if c > 0:
-            ee_s[c - 1 : c, :] = jnp.sum(full * gst_s[c], axis=0, keepdims=True)
-    last = last_s[...] + jnp.exp(before) * inc_s[...]
-    ee_s[blocks - 1 : blocks, :] = jnp.sum(last * gst_s[blocks], axis=0, keepdims=True)
-
     zero = jnp.zeros((BLK, lanes), BF16)
     lane_id = lax.broadcasted_iota(jnp.int32, (BLK, lanes), 1)
     yy_s[...] = jnp.zeros_like(yy_s)
@@ -392,81 +370,87 @@
         second = jnp.sum(jnp.where(first_head, 0.0, a), axis=1, keepdims=True)
         ref[...] = jnp.where(lane_id == c, first, jnp.where(lane_id == blocks + c, second, ref[...]))
 
-    def others(c):
+    def split_heads(a):
+        return jnp.concatenate([jnp.where(first_head, a, zero), jnp.where(first_head, zero, a)], axis=0)
+
+    def span_only(c):
         rows = block_rows(c)
+        pair = pl.ds(pl.multiple_of(c * 2 * BLK, 2 * BLK), 2 * BLK)
         q, k = q_v[:, rows], k_v[:, rows]
-        dy, v, u, er, te = dy_s[rows, :], v_s[rows, :], u_s[rows, :], er_s[rows, :], te_s[rows, :]
+        v = v_s[rows, :]
         sv = se_s[rows, :] * v
         sv_high, sv_low = halves(sv)
-
-        def split_heads(a, axis):
-            return jnp.concatenate([jnp.where(first_head, a, zero), jnp.where(first_head, zero, a)], axis=axis)
-
-        spread = jnp.concatenate([split_heads(sv_high, 0), split_heads(sv_low, 0)], axis=1)
-        mixed = folded(nn(tm_s[rows, :].astype(BF16), spread)) + er * folded(tn(q, both(sst_s[c])))
+        by_head = split_heads(sv_high)
+        m_s[rows, :] = folded(tn(tm_s[pair, :], jnp.concatenate([by_head, split_heads(sv_low)], axis=1)))
+        d = nt(by_head, dy_s[rows, :].astype(BF16)) * lm_s[pair, :]
+        d_high, d_low = halves(d[0:BLK, :] + d[BLK : 2 * BLK, :])
+        kg_ref[:, rows] = nt(
+            jnp.concatenate([q, q], axis=1), jnp.concatenate([d_high, d_low], axis=1)
+        ) + nt(gst_s[c + 1].astype(BF16), (te_s[rows, :] * sv).astype(BF16))
+        qg_ref[:, rows] = nn(jnp.concatenate([k, k], axis=1), jnp.concatenate([d_high, d_low], axis=0))
+        keep_head_sums(dd_s, c, v * u_s[rows, :])
+
+    def with_entering(c):
+        rows = block_rows(c)
+        dy, er = dy_s[rows, :], er_s[rows, :]
+        mixed = m_s[rows, :] + er * folded(tn(q_v[:, rows], both(sst_s[c])))
         gate = gate_v[rows, :].astype(F32)
         sig = sigmoid(gate)
         gg_ref[rows, :] = cot_v[rows, :].astype(F32) * mixed * sig * (1.0 + gate * (1.0 - sig))
-        dp = nt(split_heads(dy.astype(BF16), 0), sv_high)
-        d = dp[0:BLK, :] * lm_s[rows, 0:BLK] + dp[BLK : 2 * BLK, :] * lm_s[rows, BLK : 2 * BLK]
-        d_high, d_low = halves(d)
-        qg_ref[:, rows] = nt(
-            jnp.concatenate([k, k], axis=1), jnp.concatenate([d_high, d_low], axis=1)
-        ) + nt(sst_s[c].astype(BF16), (er * dy).astype(BF16))
-        kg_ref[:, rows] = nn(
-            jnp.concatenate([q, q], axis=1), jnp.concatenate([d_high, d_low], axis=0)
-        ) + nt(gst_s[c + 1].astype(BF16), (te * sv).astype(BF16))
+        qg_ref[:, rows] = qg_ref[:, rows] + nt(sst_s[c].astype(BF16), (er * dy).astype(BF16))
         keep_head_sums(yy_s, c, dy * mixed)
-        keep_head_sums(dd_s, c, v * u)
-
-    for_blocks(0, blocks, 2, others)
-    ends = ee_s[...]
-    end_cols = jnp.concatenate(
-        [
-            jnp.sum(ends[:, 0:HEAD], axis=1, keepdims=True),
-            jnp.sum(ends[:, HEAD:lanes], axis=1, keepdims=True),
-        ],
-        axis=0,
-    )
-    direct = dd_s[...].T[0 : 2 * blocks, :]
-    log_grad = nn(yy_s[...].T[0 : 2 * blocks, :] - step * direct, lower.astype(F32), HIGHEST) + end_cols
-    decay_grad = (direct - rate * log_grad) * sigmoid(pre)
-    for h in range(2):
-        for c in range(blocks):
-            dg_ref[h : h + 1, c * BLK : (c + 1) * BLK] = decay_grad[h * blocks + c : h * blocks + c + 1, :]
+
+    steps = (4, blocks // 2, blocks * 3 // 4) if blocks >= 16 else (1, blocks // 2, blocks // 2)
+    for_blocks(0, steps[1], steps[0], span_only)
+    for direction, lane in ((-1, 2), (1, 0), (1, 1), (-1, 3)):
+        for half in range(2):
+            far_copy(half, lane).wait_recv()
+            ref = piece(half, 1 if direction == 1 else 3, lane)
+            ref[...] = ref[...] + far_r[half * RING + lane]
+            near_copy(half, direction, lane).start()
+
+    own_state, own_state_log, ring_state, ring_log = row_sum(srow, ss_sem, sr_sem, (0, 1, 2, 3))
+    message(scol, mz, ring_state, ring_log)
+    for target in range(1, RING):
+
+        @pl.when(target > mz)
+        def _(target=target):
+            col_copy(scol, ss2_sem, sr2_sem, mz, target).start()
+
+    for_blocks(steps[1], steps[2], steps[0], span_only)
 
     quarter = HEAD // 2
 
     def total_of(half, across):
-        plus, minus = (half * 2) * RING + across, (half * 2 + 1) * RING + across
-        near_copy(half, 1, across).wait_recv()
-        near_copy(half, -1, across).wait_recv()
-        return piece(half, 0, across)[...] + near_r[plus] + near_r[minus]
+        pair = half * RING + across
+        all_of(near_r.at[2 * pair : 2 * pair + 2], ns_sem.at[0], nr_sem.at[pair]).wait_recv()
+        return piece(half, 0, across)[...] + near_r[2 * pair] + near_r[2 * pair + 1]
 
     def far2_copy(half, which):
         slot = half * 2 + which
         return pltpu.make_async_remote_copy(
             src_ref=red_s.at[half * RING + 2, which * quarter : (which + 1) * quarter, :],
             dst_ref=far2_r.at[slot],
-            send_sem=f2s_sem.at[slot],
+            send_sem=f2s_sem.at[0],
             recv_sem=f2r_sem.at[slot],
             device_id={"sp": neighbour(half, 1, 1 if which == 0 else -1)},
             device_id_type=MESH,
         )
 
     def near2_copy(half, direction, which):
-        side = 0 if direction == 1 else 1
-        slot = (half * 2 + side) * 2 + which
+        pair = half * 2 + which
         return pltpu.make_async_remote_copy(
             src_ref=red_s.at[half * RING + (1 if direction == 1 else 3), which * quarter : (which + 1) * quarter, :],
-            dst_ref=near2_r.at[slot],
-            send_sem=n2s_sem.at[slot],
-            recv_sem=n2r_sem.at[slot],
+            dst_ref=near2_r.at[2 * pair + (0 if direction == 1 else 1)],
+            send_sem=n2s_sem.at[0],
+            recv_sem=n2r_sem.at[pair],
             device_id={"sp": neighbour(half, 1, direction)},
             device_id_type=MESH,
         )
 
     for across in (2, 1, 3, 0):
+        if across == 1:
+            for_blocks(steps[2], blocks, steps[0], span_only)
         for half in range(2):
             red_s[half * RING + across] = total_of(half, across)
             if across == 2:
@@ -484,14 +468,35 @@
             red_s[at, span, :] = red_s[at, span, :] + far2_r[half * 2 + which]
             near2_copy(half, direction, which).start()
 
+    inc_s[...] = jnp.zeros_like(inc_s)
+    for source in range(RING - 1):
+
+        @pl.when(source < mz)
+        def _(source=source):
+            col_copy(scol, ss2_sem, sr2_sem, source, mz).wait_recv()
+            inc_s[...] = scol[source, 0:STATE, :] + jnp.exp(scol[source, STATE : STATE + 1, :]) * inc_s[...]
+
+    inc_s[...] = own_state + jnp.exp(own_state_log) * inc_s[...]
+    before = jnp.zeros((1, lanes), F32)
+    for c in range(blocks):
+        full = sst_s[c] + jnp.exp(before) * inc_s[...]
+        sst_s[c] = full
+        before = before + rend_s[c : c + 1, :]
+        if c > 0:
+            ee_s[c - 1 : c, :] = jnp.sum(full * gst_s[c], axis=0, keepdims=True)
+    last = last_s[...] + jnp.exp(before) * inc_s[...]
+    ee_s[blocks - 1 : blocks, :] = jnp.sum(last * gst_s[blocks], axis=0, keepdims=True)
+
+    later = blocks * 3 // 4 if blocks >= 8 else blocks // 2
+    for_blocks(0, later, min(4, later), with_entering)
+
     squares = jnp.zeros((1, cols), F32)
     for half in range(2):
         for which in range(2):
-            for direction in (1, -1):
-                near2_copy(half, direction, which).wait_recv()
-            plus, minus = (half * 2) * 2 + which, (half * 2 + 1) * 2 + which
+            pair = half * 2 + which
+            all_of(near2_r.at[2 * pair : 2 * pair + 2], n2s_sem.at[0], n2r_sem.at[pair]).wait_recv()
             span = slice(which * quarter, (which + 1) * quarter)
-            done = red_s[half * RING, span, :] + near2_r[plus] + near2_r[minus]
+            done = red_s[half * RING, span, :] + near2_r[2 * pair] + near2_r[2 * pair + 1]
             red_s[half * RING, span, :] = done
             squares = squares + jnp.sum(done * done, axis=0, keepdims=True)
 
@@ -499,8 +504,8 @@
         return pltpu.make_async_remote_copy(
             src_ref=nmsg,
             dst_ref=nslots.at[source],
-            send_sem=norm_s.at[target],
-            recv_sem=norm_r.at[source],
+            send_sem=norm_s.at[0],
+            recv_sem=norm_r.at[0],
             device_id={"tp": target},
             device_id_type=MESH,
         )
@@ -508,18 +513,32 @@
     nmsg[...] = jnp.broadcast_to(squares, (8, cols))
     for off in range(1, tp_count):
         norm_copy(my_tp, lax.rem(my_tp + off, tp_count)).start()
+    for_blocks(later, blocks, min(4, blocks - later), with_entering)
+    ends = ee_s[...]
+    end_cols = jnp.concatenate(
+        [
+            jnp.sum(ends[:, 0:HEAD], axis=1, keepdims=True),
+            jnp.sum(ends[:, HEAD:lanes], axis=1, keepdims=True),
+        ],
+        axis=0,
+    )
+    direct = dd_s[...].T[0 : 2 * blocks, :]
+    log_grad = nn(yy_s[...].T[0 : 2 * blocks, :] - step * direct, lower.astype(F32), HIGHEST) + end_cols
+    decay_grad = (direct - rate * log_grad) * sigmoid(pre)
+    for h in range(2):
+        for c in range(blocks):
+            dg_ref[h : h + 1, c * BLK : (c + 1) * BLK] = decay_grad[h * blocks + c : h * blocks + c + 1, :]
     for half in range(2):
         wg_ref[:, half * HEAD : (half + 1) * HEAD] = red_s[half * RING].T
     norms = squares
+    if tp_count > 1:
+        all_of(nslots.at[0 : tp_count - 1], norm_s.at[0], norm_r.at[0]).wait_recv()
     for off in range(1, tp_count):
-        source = lax.rem(my_tp + off, tp_count)
-        norm_copy(source, my_tp).wait_recv()
-        norms = norms + nslots[source, 0:1, :]
+        norms = norms + nslots[lax.rem(my_tp + off, tp_count), 0:1, :]
     rn_ref[...] = norms
 
-    for off in range(1, RING):
-        row_copy(grow, gs_sem, gr_sem, mx, lax.rem(mx + off, RING)).wait_send()
-        row_copy(srow, ss_sem, sr_sem, mx, lax.rem(mx + off, RING)).wait_send()
+    all_of(grow.at[0 : RING - 1], gs_sem.at[0], gr_sem.at[0]).wait_send()
+    all_of(srow.at[0 : RING - 1], ss_sem.at[0], sr_sem.at[0]).wait_send()
     for target in range(RING):
 
         @pl.when(target < mz)
@@ -530,17 +549,12 @@
         def _(target=target):
             col_copy(scol, ss2_sem, sr2_sem, mz, target).wait_send()
 
-    for half in range(2):
-        for across in range(RING):
-            far_copy(half, across).wait_send()
-            for direction in (1, -1):
-                near_copy(half, direction, across).wait_send()
-        for which in range(2):
-            far2_copy(half, which).wait_send()
-            for direction in (1, -1):
-                near2_copy(half, direction, which).wait_send()
-    for off in range(1, tp_count):
-        norm_copy(my_tp, lax.rem(my_tp + off, tp_count)).wait_send()
+    all_of(far_r, fs_sem.at[0], fr_sem.at[0]).wait_send()
+    all_of(near_r, ns_sem.at[0], nr_sem.at[0]).wait_send()
+    all_of(far2_r, f2s_sem.at[0], f2r_sem.at[0]).wait_send()
+    all_of(near2_r, n2s_sem.at[0], n2r_sem.at[0]).wait_send()
+    if tp_count > 1:
+        all_of(nslots.at[0 : tp_count - 1], norm_s.at[0], norm_r.at[0]).wait_send()
 
 
 def put_out(*refs):
@@ -561,10 +575,11 @@
     dma = lambda *shape: pltpu.SemaphoreType.DMA(shape)
     state_msg = (STATE + 8, lanes)
     scratch = [
+        vmem((tokens, lanes)),
         vmem((tokens, width), BF16), vmem((width, lanes), BF16), vmem((STATE, tokens), BF16), vmem((STATE, tokens), BF16),
         vmem((2, tokens)), pltpu.SMEM((2,), F32), vmem((tokens, lanes), BF16), vmem((tokens, lanes), BF16),
         vmem((2 * blocks, BLK)), vmem((BLK, BLK)), vmem((blocks, lanes)),
-        vmem((tokens, lanes)), vmem((tokens, 2 * BLK)), vmem((tokens, 2 * BLK)), vmem((tokens, lanes)),
+        vmem((tokens, lanes)), vmem((2 * tokens, BLK), BF16), vmem((2 * tokens, BLK)), vmem((tokens, lanes)),
         vmem((tokens, lanes)), vmem((tokens, lanes)), vmem((tokens, lanes)), vmem((tokens, lanes)), vmem((tokens, lanes)),
         vmem((blocks + 1, STATE, lanes)), vmem((blocks, STATE, lanes)), vmem((blocks, STATE, lanes)),
         vmem((STATE, lanes)), vmem((STATE, lanes)), vmem((lanes, tokens), BF16),
@@ -573,8 +588,8 @@
         vmem((sp_count, lanes, cols)), vmem((8, HEAD, cols)), vmem((16, HEAD, cols)), vmem((8, HEAD, cols)),
         vmem((4, HEAD // 2, cols)), vmem((8, HEAD // 2, cols)),
         vmem((8, cols)), vmem((tp_count, 8, cols)),
-        dma(7), dma(max(2, tokens // (4 * BLK))), *(dma(RING) for _ in range(8)),
-        dma(8), dma(8), dma(16), dma(16), dma(4), dma(4), dma(8), dma(8), dma(tp_count), dma(tp_count),
+        dma(7), dma(max(2, tokens // (4 * BLK))), *(dma(1) for _ in range(4)), *(dma(RING) for _ in range(4)),
+        dma(1), dma(8), dma(1), dma(8), dma(1), dma(4), dma(1), dma(4), dma(1), dma(1),
     ]
     hbm = pl.BlockSpec(memory_space=pltpu.HBM)
     in_vmem = pl.BlockSpec(memory_space=pltpu.VMEM)

time: 49.3 us -> 44 us (0.89)
  Pallas kernels: 48.5 us -> 43.2 us
    pallas_call x1, Pallas kernels: 47.1 us -> 41.8 us  [shards(): pl.pallas_call(functools.partial(mixer, sp_count, tp_count), out_shape=(j...]
where the time goes in v2:
time: 44 us; the launch traced here: 43.8 us
  Pallas kernels  43.2 us (98%)
  between operations  0.64 us (1%)
    pallas_call x1, Pallas kernels, shards(): pl.pallas_call(functools.partial(mixer, sp_count, tp_count), out_shape=(j...  41.8 us
    pallas_call x1, Pallas kernels, shards(): pl.pallas_call(put_out, out_shape=tuple((jax.ShapeDtypeStruct(o.shape, o....  1.41 us

profile of v2, /device:TPU:1, one launch (start us, length us, event | category | flops | bytes accessed | tf_op | source)
XLA Modules:
  0.0 43.8 jit_solution(6478427180747610437)
XLA Ops:
  0.6 41.8 %mixer.1 = (f32[64,2048]{1,0:T(8,128)S(1)}, f32[64,2048]{1,0:T(8,128)S(1)}, f32[2,2048]{1,0:T(2,128)S(1)}, f32[2048,128]{1,0:T(8,128)S(1)}, f32[256,128]{1,0:T(8,128)S(1)}, /*index=5*/f32[1,256]{1,0:T(1,128)S(1)}) custom-call(bf16[2048,4096]{1,0:T(8,128)(2,1)} %x_hbm.1, bf16[4096,128]{1,0:T(8,128)(2,1)} %w_hbm.1, bf16[64,2048]{1,0:T(8,128)(2,1)} %bitcast.5, ...), custom_call_target="tpu_custom_call" | custom-call | tf_op jit(solution)/shard_map/mixer/pallas_call | solution.py:596
  42.4 1.4 %put_out.1 = (f32[64,2048]{1,0:T(8,128)}, f32[64,2048]{1,0:T(8,128)}, f32[2,2048]{1,0:T(2,128)}, f32[2048,128]{1,0:T(8,128)}, f32[256,128]{1,0:T(8,128)}, /*index=5*/f32[1,256]{1,0:T(1,128)}) custom-call(f32[64,2048]{1,0:T(8,128)S(1)} %get-tuple-element.18.refs_0_, f32[64,2048]{1,0:T(8,128)S(1)} %get-tuple-element.19.refs_1_, ...), custom_call_target="tpu_custom_call" | custom-call | tf_op jit(solution)/shard_map/put_out/pallas_call | solution.py:618

commit v3 on v2

--- a/solution.py
+++ b/solution.py
@@ -63,15 +63,15 @@
     kg_ref, qg_ref, dg_ref, gg_ref, wg_ref, rn_ref,
     m_s,
     x_v, w_v, k_v, q_v, pre_v, rate_ref, gate_v, cot_v,
-    rows_s, stack_s, rend_s,
+    rows_s, stack_s, rend_s, fend_s,
     dy_s, tm_s, lm_s, er_s, te_s, se_s, p_s, v_s, u_s,
     gst_s, sst_s, bs_s, out_s, inc_s, vgt_s,
     yy_s, dd_s, ee_s,
     last_s, grow, gcol, srow, scol,
-    part, far_r, near_r, red_s, far2_r, near2_r,
+    part, far_r, near_r, red_s, second_r,
     nmsg, nslots,
     in_sem, x_sem, gs_sem, gr_sem, ss_sem, sr_sem, gs2_sem, gr2_sem, ss2_sem, sr2_sem,
-    fs_sem, fr_sem, ns_sem, nr_sem, f2s_sem, f2r_sem, n2s_sem, n2r_sem, norm_s, norm_r,
+    far_s, far_sem, near_s, near_sem, second_s, second_sem, norm_s, norm_r,
 ):
     tokens, width = x_v.shape
     blocks = tokens // BLK
@@ -125,21 +125,35 @@
     upper = sq_row <= sq_col
     lower = sq_row >= sq_col
     run = nn(-rate * step, (sq_row <= sq_col).astype(F32), HIGHEST)
-    stack_s[...] = jnp.zeros_like(stack_s)
+    if 8 * blocks < BLK:
+        stack_s[...] = jnp.zeros_like(stack_s)
     stack_s[0 : 2 * blocks, :] = run
     stack_s[2 * blocks : 4 * blocks, :] = step
+    stack_s[4 * blocks : 6 * blocks, :] = jnp.exp(run)
+    stack_s[6 * blocks : 8 * blocks, :] = jnp.exp(run[:, BLK - 1 : BLK] - run)
     turned = stack_s[...].T
+    rend = jnp.where(
+        lax.broadcasted_iota(jnp.int32, (blocks, lanes), 1) < HEAD,
+        run[0:blocks, BLK - 1 : BLK],
+        run[blocks : 2 * blocks, BLK - 1 : BLK],
+    )
+    rend_s[...] = rend
+    fend_s[...] = jnp.exp(rend)
     first_head = lax.broadcasted_iota(jnp.int32, (BLK, lanes), 1) < HEAD
     for copy in small[2:6]:
         copy.wait()
     small[6].start()
-    for i in range(xchunks):
-        x_copy(i).start()
+    x_copy(0).start()
 
     def block_rows(c):
-        return pl.ds(pl.multiple_of(c * BLK, BLK), BLK)
+        return pl.ds(c * BLK if isinstance(c, int) else pl.multiple_of(c * BLK, BLK), BLK)
 
     def for_blocks(start, stop, unroll, body):
+        if unroll == stop - start:
+            for c in range(start, stop):
+                body(c)
+            return
+
         def step_of(i, carry):
             for b in range(unroll):
                 body(start + i * unroll + b)
@@ -148,26 +162,23 @@
         lax.fori_loop(0, (stop - start) // unroll, step_of, 0)
 
     def columns_of(c, kinds):
-        rolled = pltpu.roll(turned, lax.rem(BLK - c, BLK), 1)
-        return [jnp.broadcast_to(rolled[:, i * blocks : i * blocks + 1], (BLK, BLK)) for i in kinds]
+        return [jnp.broadcast_to(turned[:, i * blocks + c : i * blocks + c + 1], (BLK, BLK)) for i in kinds]
 
     def prepare(c):
         rows = block_rows(c)
-        running = jnp.where(first_head, *columns_of(c, (0, 1)))
-        er = jnp.exp(running)
+        er = jnp.where(first_head, *columns_of(c, (4, 5)))
         er_s[rows, :] = er
-        rend_s[pl.ds(c, 1), :] = running[BLK - 1 : BLK, :]
         gate = gate_v[rows, :].astype(F32)
         dy = cot_v[rows, :].astype(F32) * gate * sigmoid(gate)
         dy_s[rows, :] = dy
         bs_s[c] = folded(nn(q_v[:, rows], both(er * dy)))
 
-    for_blocks(0, blocks, min(8, blocks), prepare)
+    for_blocks(0, blocks, blocks, prepare)
     grad = jnp.zeros((STATE, lanes), F32)
     total = jnp.zeros((1, lanes), F32)
     for c in reversed(range(blocks)):
         end = rend_s[c : c + 1, :]
-        grad = jnp.exp(end) * grad + bs_s[c]
+        grad = fend_s[c : c + 1, :] * grad + bs_s[c]
         total = total + end
         gst_s[c] = grad
     def message(ref, at, value, log):
@@ -222,8 +233,6 @@
         return own, own_log, acc, log
 
     message(grow, mx, grad, total)
-    pl.semaphore_wait(barrier, 2 * (RING - 1) + tp_count - 1)
-    send_row(grow, gs_sem, gr_sem)
 
     def project(i):
         x_copy(i).wait()
@@ -232,19 +241,18 @@
 
     def local(c):
         rows = block_rows(c)
-        col = columns_of(c, range(4))
-        pair = pl.ds(pl.multiple_of(c * 2 * BLK, 2 * BLK), 2 * BLK)
+        col = columns_of(c, (0, 1, 2, 3, 6, 7))
+        pair = pl.ds(c * 2 * BLK, 2 * BLK)
         scores = tn(k_v[:, rows], q_v[:, rows])
         decay = jnp.concatenate(
             [
-                jnp.exp(jnp.where(upper, stack_s[pl.ds(h * blocks + c, 1), :] - col[h], -1e30))
+                jnp.exp(jnp.where(upper, stack_s[h * blocks + c : h * blocks + c + 1, :] - col[h], -1e30))
                 for h in range(2)
             ],
             axis=0,
         )
         lm_s[pair, :] = decay
-        running = jnp.where(first_head, col[0], col[1])
-        te_s[rows, :] = jnp.exp(running[BLK - 1 : BLK, :] - running)
+        te_s[rows, :] = jnp.where(first_head, col[4], col[5])
         se_s[rows, :] = jnp.where(first_head, col[2], col[3])
         dy_high, dy_low = halves(dy_s[rows, :])
         t_high, t_low = halves(jnp.concatenate([scores, scores], axis=0) * decay)
@@ -259,13 +267,22 @@
         v_s[rows, :] = v
         bs_s[c] = folded(nn(k_v[:, rows], both(te_s[rows, :] * se_s[rows, :] * v)))
 
-    for_blocks(0, blocks, min(4, blocks), local)
+    x_copy(1).start()
+    for c in range(blocks):
+        if c == blocks // 4:
+            pl.semaphore_wait(barrier, 2 * (RING - 1) + tp_count - 1)
+            send_row(grow, gs_sem, gr_sem)
+        if c == blocks // 2:
+            for i in range(2, xchunks):
+                x_copy(i).start()
+        local(c)
     small[6].wait()
 
     def chunk(i, carry):
         project(i)
         return carry
 
+    chunk(0, 0)
     own_grad, own_log, ring_grad, ring_log = row_sum(grow, gs_sem, gr_sem, (3, 2, 1, 0))
     message(gcol, mz, ring_grad, ring_log)
     for target in (1, 0, 2):
@@ -274,12 +291,12 @@
         def _(target=target):
             col_copy(gcol, gs2_sem, gr2_sem, mz, target).start()
 
-    lax.fori_loop(0, xchunks, chunk, 0)
-    for_blocks(0, blocks, min(4, blocks), with_values)
+    lax.fori_loop(1, xchunks, chunk, 0)
+    for_blocks(0, blocks, blocks, with_values)
     state = jnp.zeros((STATE, lanes), F32)
     for c in range(blocks):
         sst_s[c] = state
-        state = jnp.exp(rend_s[c : c + 1, :]) * state + bs_s[c]
+        state = fend_s[c : c + 1, :] * state + bs_s[c]
     last_s[...] = state
     message(srow, mx, state, total)
     send_row(srow, ss_sem, sr_sem)
@@ -308,42 +325,49 @@
         vg = se_s[rows, :] * u * sig * (1.0 + projected * (1.0 - sig))
         vgt_s[:, rows] = vg.astype(BF16).T
 
-    for_blocks(0, blocks, min(4, blocks), value_gradient)
+    for_blocks(0, blocks, blocks, value_gradient)
 
     def owner(dz, dx):
         return lax.rem(mz + dz, RING) * RING + lax.rem(mx + dx, RING)
 
-    def neighbour(half, stage, direction):
-        if half == stage:
-            return lax.rem(mz + direction + RING, RING) * RING + mx
-        return mz * RING + lax.rem(mx + direction + RING, RING)
-
-    def half_of(half, dz, dx):
+    def on_axis(axis, dist):
+        if axis == 0:
+            return lax.rem(mz + dist, RING) * RING + mx
+        return mz * RING + lax.rem(mx + dist, RING)
+
+    def piece(half, dist, across):
+        dz, dx = (dist, across) if half == 0 else (across, dist)
         return part.at[owner(dz, dx), half * HEAD : (half + 1) * HEAD, :]
 
-    def piece(half, dist, across):
-        return half_of(half, dist, across) if half == 0 else half_of(half, across, dist)
-
     def far_copy(half, across):
-        direction = 1 if across < 2 else -1
-        slot = half * RING + across
+        lane = half * RING + across
         return pltpu.make_async_remote_copy(
             src_ref=piece(half, 2, across),
-            dst_ref=far_r.at[slot],
-            send_sem=fs_sem.at[0],
-            recv_sem=fr_sem.at[slot],
-            device_id={"sp": neighbour(half, 0, direction)},
+            dst_ref=far_r.at[lane],
+            send_sem=far_s.at[0],
+            recv_sem=far_sem.at[lane],
+            device_id={"sp": on_axis(half, 1 if across < 2 else 3)},
             device_id_type=MESH,
         )
 
-    def near_copy(half, direction, across):
-        pair = half * RING + across
+    def near_copy(half, dist, across):
+        lane = half * RING + across
         return pltpu.make_async_remote_copy(
-            src_ref=piece(half, 1 if direction == 1 else 3, across),
-            dst_ref=near_r.at[2 * pair + (0 if direction == 1 else 1)],
-            send_sem=ns_sem.at[0],
-            recv_sem=nr_sem.at[pair],
-            device_id={"sp": neighbour(half, 0, direction)},
+            src_ref=piece(half, dist, across),
+            dst_ref=near_r.at[2 * lane + (0 if dist == 1 else 1)],
+            send_sem=near_s.at[0],
+            recv_sem=near_sem.at[lane],
+            device_id={"sp": on_axis(half, dist)},
+            device_id_type=MESH,
+        )
+
+    def second_copy(half, across):
+        return pltpu.make_async_remote_copy(
+            src_ref=red_s.at[half * RING + across],
+            dst_ref=second_r.at[half * (RING - 1) + across - 1],
+            send_sem=second_s.at[0],
+            recv_sem=second_sem.at[half],
+            device_id={"sp": on_axis(1 - half, across)},
             device_id_type=MESH,
         )
 
@@ -356,10 +380,8 @@
             for half, dist, across in ((0, dz, dx), (1, dx, dz)):
                 if dist == 2:
                     far_copy(half, across).start()
-                elif dist == 1 and across >= 2:
-                    near_copy(half, 1, across).start()
-                elif dist == 3 and across < 2:
-                    near_copy(half, -1, across).start()
+                elif (dist, across < 2) in ((1, False), (3, True)):
+                    near_copy(half, dist, across).start()
     zero = jnp.zeros((BLK, lanes), BF16)
     lane_id = lax.broadcasted_iota(jnp.int32, (BLK, lanes), 1)
     yy_s[...] = jnp.zeros_like(yy_s)
@@ -402,13 +424,12 @@
 
     steps = (4, blocks // 2, blocks * 3 // 4) if blocks >= 16 else (1, blocks // 2, blocks // 2)
     for_blocks(0, steps[1], steps[0], span_only)
-    for direction, lane in ((-1, 2), (1, 0), (1, 1), (-1, 3)):
+    for dist, across in ((3, 2), (1, 0), (1, 1), (3, 3)):
         for half in range(2):
-            far_copy(half, lane).wait_recv()
-            ref = piece(half, 1 if direction == 1 else 3, lane)
-            ref[...] = ref[...] + far_r[half * RING + lane]
-            near_copy(half, direction, lane).start()
-
+            far_copy(half, across).wait_recv()
+            ref = piece(half, dist, across)
+            ref[...] = ref[...] + far_r[half * RING + across]
+            near_copy(half, dist, across).start()
     own_state, own_state_log, ring_state, ring_log = row_sum(srow, ss_sem, sr_sem, (0, 1, 2, 3))
     message(scol, mz, ring_state, ring_log)
     for target in range(1, RING):
@@ -418,55 +439,16 @@
             col_copy(scol, ss2_sem, sr2_sem, mz, target).start()
 
     for_blocks(steps[1], steps[2], steps[0], span_only)
-
-    quarter = HEAD // 2
-
-    def total_of(half, across):
-        pair = half * RING + across
-        all_of(near_r.at[2 * pair : 2 * pair + 2], ns_sem.at[0], nr_sem.at[pair]).wait_recv()
-        return piece(half, 0, across)[...] + near_r[2 * pair] + near_r[2 * pair + 1]
-
-    def far2_copy(half, which):
-        slot = half * 2 + which
-        return pltpu.make_async_remote_copy(
-            src_ref=red_s.at[half * RING + 2, which * quarter : (which + 1) * quarter, :],
-            dst_ref=far2_r.at[slot],
-            send_sem=f2s_sem.at[0],
-            recv_sem=f2r_sem.at[slot],
-            device_id={"sp": neighbour(half, 1, 1 if which == 0 else -1)},
-            device_id_type=MESH,
-        )
-
-    def near2_copy(half, direction, which):
-        pair = half * 2 + which
-        return pltpu.make_async_remote_copy(
-            src_ref=red_s.at[half * RING + (1 if direction == 1 else 3), which * quarter : (which + 1) * quarter, :],
-            dst_ref=near2_r.at[2 * pair + (0 if direction == 1 else 1)],
-            send_sem=n2s_sem.at[0],
-            recv_sem=n2r_sem.at[pair],
-            device_id={"sp": neighbour(half, 1, direction)},
-            device_id_type=MESH,
-        )
 
     for across in (2, 1, 3, 0):
         if across == 1:
             for_blocks(steps[2], blocks, steps[0], span_only)
         for half in range(2):
-            red_s[half * RING + across] = total_of(half, across)
-            if across == 2:
-                far2_copy(half, 0).start()
-                far2_copy(half, 1).start()
-            elif across == 1:
-                near2_copy(half, 1, 1).start()
-            elif across == 3:
-                near2_copy(half, -1, 0).start()
-    for half in range(2):
-        for direction, which in ((1, 0), (-1, 1)):
-            far2_copy(half, which).wait_recv()
-            at = half * RING + (1 if direction == 1 else 3)
-            span = slice(which * quarter, (which + 1) * quarter)
-            red_s[at, span, :] = red_s[at, span, :] + far2_r[half * 2 + which]
-            near2_copy(half, direction, which).start()
+            lane = half * RING + across
+            all_of(near_r.at[2 * lane : 2 * lane + 2], near_s.at[0], near_sem.at[lane]).wait_recv()
+            red_s[lane] = piece(half, 0, across)[...] + near_r[2 * lane] + near_r[2 * lane + 1]
+            if across != 0:
+                second_copy(half, across).start()
 
     inc_s[...] = jnp.zeros_like(inc_s)
     for source in range(RING - 1):
@@ -492,13 +474,11 @@
 
     squares = jnp.zeros((1, cols), F32)
     for half in range(2):
-        for which in range(2):
-            pair = half * 2 + which
-            all_of(near2_r.at[2 * pair : 2 * pair + 2], n2s_sem.at[0], n2r_sem.at[pair]).wait_recv()
-            span = slice(which * quarter, (which + 1) * quarter)
-            done = red_s[half * RING, span, :] + near2_r[2 * pair] + near2_r[2 * pair + 1]
-            red_s[half * RING, span, :] = done
-            squares = squares + jnp.sum(done * done, axis=0, keepdims=True)
+        at = half * (RING - 1)
+        all_of(second_r.at[at : at + RING - 1], second_s.at[0], second_sem.at[half]).wait_recv()
+        done = red_s[half * RING] + second_r[at] + second_r[at + 1] + second_r[at + 2]
+        red_s[half * RING] = done
+        squares = squares + jnp.sum(done * done, axis=0, keepdims=True)
 
     def norm_copy(source, target):
         return pltpu.make_async_remote_copy(
@@ -549,10 +529,9 @@
         def _(target=target):
             col_copy(scol, ss2_sem, sr2_sem, mz, target).wait_send()
 
-    all_of(far_r, fs_sem.at[0], fr_sem.at[0]).wait_send()
-    all_of(near_r, ns_sem.at[0], nr_sem.at[0]).wait_send()
-    all_of(far2_r, f2s_sem.at[0], f2r_sem.at[0]).wait_send()
-    all_of(near2_r, n2s_sem.at[0], n2r_sem.at[0]).wait_send()
+    all_of(far_r, far_s.at[0], far_sem.at[0]).wait_send()
+    all_of(near_r, near_s.at[0], near_sem.at[0]).wait_send()
+    all_of(second_r, second_s.at[0], second_sem.at[0]).wait_send()
     if tp_count > 1:
         all_of(nslots.at[0 : tp_count - 1], norm_s.at[0], norm_r.at[0]).wait_send()
 
@@ -578,7 +557,7 @@
         vmem((tokens, lanes)),
         vmem((tokens, width), BF16), vmem((width, lanes), BF16), vmem((STATE, tokens), BF16), vmem((STATE, tokens), BF16),
         vmem((2, tokens)), pltpu.SMEM((2,), F32), vmem((tokens, lanes), BF16), vmem((tokens, lanes), BF16),
-        vmem((2 * blocks, BLK)), vmem((BLK, BLK)), vmem((blocks, lanes)),
+        vmem((2 * blocks, BLK)), vmem((BLK, BLK)), vmem((blocks, lanes)), vmem((blocks, lanes)),
         vmem((tokens, lanes)), vmem((2 * tokens, BLK), BF16), vmem((2 * tokens, BLK)), vmem((tokens, lanes)),
         vmem((tokens, lanes)), vmem((tokens, lanes)), vmem((tokens, lanes)), vmem((tokens, lanes)), vmem((tokens, lanes)),
         vmem((blocks + 1, STATE, lanes)), vmem((blocks, STATE, lanes)), vmem((blocks, STATE, lanes)),
@@ -586,10 +565,10 @@
         vmem((BLK, lanes)), vmem((BLK, lanes)), vmem((blocks, lanes)),
         vmem((STATE, lanes)), *(vmem((RING, *state_msg)) for _ in range(4)),
         vmem((sp_count, lanes, cols)), vmem((8, HEAD, cols)), vmem((16, HEAD, cols)), vmem((8, HEAD, cols)),
-        vmem((4, HEAD // 2, cols)), vmem((8, HEAD // 2, cols)),
+        vmem((6, HEAD, cols)),
         vmem((8, cols)), vmem((tp_count, 8, cols)),
         dma(7), dma(max(2, tokens // (4 * BLK))), *(dma(1) for _ in range(4)), *(dma(RING) for _ in range(4)),
-        dma(1), dma(8), dma(1), dma(8), dma(1), dma(4), dma(1), dma(4), dma(1), dma(1),
+        dma(1), dma(8), dma(1), dma(8), dma(1), dma(2), dma(1), dma(1),
     ]
     hbm = pl.BlockSpec(memory_space=pltpu.HBM)
     in_vmem = pl.BlockSpec(memory_space=pltpu.VMEM)

time: 44 us -> 40.4 us (0.918)
  Pallas kernels: 43.2 us -> 39.6 us
    pallas_call x1, Pallas kernels: 41.8 us -> 38.2 us  [shards(): pl.pallas_call(functools.partial(mixer, sp_count, tp_count), out_shape=(j...]
where the time goes in v3:
time: 40.4 us; the launch traced here: 40.2 us
  Pallas kernels  39.6 us (98%)
  between operations  0.64 us (2%)
    pallas_call x1, Pallas kernels, shards(): pl.pallas_call(functools.partial(mixer, sp_count, tp_count), out_shape=(j...  38.2 us
    pallas_call x1, Pallas kernels, shards(): pl.pallas_call(put_out, out_shape=tuple((jax.ShapeDtypeStruct(o.shape, o....  1.41 us

profile of v3, /device:TPU:1, one launch (start us, length us, event | category | flops | bytes accessed | tf_op | source)
XLA Modules:
  0.0 40.2 jit_solution(4863218173980864503)
XLA Ops:
  0.6 38.2 %mixer.1 = (f32[64,2048]{1,0:T(8,128)S(1)}, f32[64,2048]{1,0:T(8,128)S(1)}, f32[2,2048]{1,0:T(2,128)S(1)}, f32[2048,128]{1,0:T(8,128)S(1)}, f32[256,128]{1,0:T(8,128)S(1)}, /*index=5*/f32[1,256]{1,0:T(1,128)S(1)}) custom-call(bf16[2048,4096]{1,0:T(8,128)(2,1)} %x_hbm.1, bf16[4096,128]{1,0:T(8,128)(2,1)} %w_hbm.1, bf16[64,2048]{1,0:T(8,128)(2,1)} %bitcast.5, ...), custom_call_target="tpu_custom_call" | custom-call | tf_op jit(solution)/shard_map/mixer/pallas_call | solution.py:575
  38.8 1.4 %put_out.1 = (f32[64,2048]{1,0:T(8,128)}, f32[64,2048]{1,0:T(8,128)}, f32[2,2048]{1,0:T(2,128)}, f32[2048,128]{1,0:T(8,128)}, f32[256,128]{1,0:T(8,128)}, /*index=5*/f32[1,256]{1,0:T(1,128)}) custom-call(f32[64,2048]{1,0:T(8,128)S(1)} %get-tuple-element.18.refs_0_, f32[64,2048]{1,0:T(8,128)S(1)} %get-tuple-element.19.refs_1_, ...), custom_call_target="tpu_custom_call" | custom-call | tf_op jit(solution)/shard_map/put_out/pallas_call | solution.py:597

commit v4 on v3

--- a/solution.py
+++ b/solution.py
@@ -239,6 +239,8 @@
         rows = pl.ds(pl.multiple_of(i * xrows, xrows), xrows)
         p_s[rows, :] = nn(x_v[rows, :], w_v[...]).astype(BF16).astype(F32)
 
+    zero = jnp.zeros((BLK, lanes), BF16)
+
     def local(c):
         rows = block_rows(c)
         col = columns_of(c, (0, 1, 2, 3, 6, 7))
@@ -257,7 +259,14 @@
         dy_high, dy_low = halves(dy_s[rows, :])
         t_high, t_low = halves(jnp.concatenate([scores, scores], axis=0) * decay)
         tm_s[pair, :] = t_high
-        u = folded(nn(t_high, jnp.concatenate([dy_high, dy_low], axis=1))) + nn(t_low, dy_high)
+        u = folded(
+            nn(
+                jnp.concatenate([t_high, t_low], axis=1),
+                jnp.concatenate(
+                    [jnp.concatenate([dy_high, dy_low], axis=1), jnp.concatenate([dy_high, zero], axis=1)], axis=0
+                ),
+            )
+        )
         u_s[rows, :] = jnp.where(first_head, u[0:BLK, :], u[BLK : 2 * BLK, :])
 
     def with_values(c):
@@ -269,7 +278,7 @@
 
     x_copy(1).start()
     for c in range(blocks):
-        if c == blocks // 4:
+        if c == 0:
             pl.semaphore_wait(barrier, 2 * (RING - 1) + tp_count - 1)
             send_row(grow, gs_sem, gr_sem)
         if c == blocks // 2:
@@ -382,7 +391,6 @@
                     far_copy(half, across).start()
                 elif (dist, across < 2) in ((1, False), (3, True)):
                     near_copy(half, dist, across).start()
-    zero = jnp.zeros((BLK, lanes), BF16)
     lane_id = lax.broadcasted_iota(jnp.int32, (BLK, lanes), 1)
     yy_s[...] = jnp.zeros_like(yy_s)
     dd_s[...] = jnp.zeros_like(dd_s)

time: 40.4 us -> 39.2 us (0.970)
  Pallas kernels: 39.6 us -> 38.4 us
    pallas_call x1, Pallas kernels: 38.2 us -> 37 us  [shards(): pl.pallas_call(functools.partial(mixer, sp_count, tp_count), out_shape=(j...]
where the time goes in v4:
time: 39.2 us; the launch traced here: 39.1 us
  Pallas kernels  38.4 us (98%)
  between operations  0.64 us (2%)
    pallas_call x1, Pallas kernels, shards(): pl.pallas_call(functools.partial(mixer, sp_count, tp_count), out_shape=(j...  37 us
    pallas_call x1, Pallas kernels, shards(): pl.pallas_call(put_out, out_shape=tuple((jax.ShapeDtypeStruct(o.shape, o....  1.41 us

profile of v4, /device:TPU:1, one launch (start us, length us, event | category | flops | bytes accessed | tf_op | source)
XLA Modules:
  0.0 39.1 jit_solution(12470030693840814668)
XLA Ops:
  0.6 37.0 %mixer.1 = (f32[64,2048]{1,0:T(8,128)S(1)}, f32[64,2048]{1,0:T(8,128)S(1)}, f32[2,2048]{1,0:T(2,128)S(1)}, f32[2048,128]{1,0:T(8,128)S(1)}, f32[256,128]{1,0:T(8,128)S(1)}, /*index=5*/f32[1,256]{1,0:T(1,128)S(1)}) custom-call(bf16[2048,4096]{1,0:T(8,128)(2,1)} %x_hbm.1, bf16[4096,128]{1,0:T(8,128)(2,1)} %w_hbm.1, bf16[64,2048]{1,0:T(8,128)(2,1)} %bitcast.5, ...), custom_call_target="tpu_custom_call" | custom-call | tf_op jit(solution)/shard_map/mixer/pallas_call | solution.py:583
  37.6 1.4 %put_out.1 = (f32[64,2048]{1,0:T(8,128)}, f32[64,2048]{1,0:T(8,128)}, f32[2,2048]{1,0:T(2,128)}, f32[2048,128]{1,0:T(8,128)}, f32[256,128]{1,0:T(8,128)}, /*index=5*/f32[1,256]{1,0:T(1,128)}) custom-call(f32[64,2048]{1,0:T(8,128)S(1)} %get-tuple-element.18.refs_0_, f32[64,2048]{1,0:T(8,128)S(1)} %get-tuple-element.19.refs_1_, ...), custom_call_target="tpu_custom_call" | custom-call | tf_op jit(solution)/shard_map/put_out/pallas_call | solution.py:605
